TPU v7x, 256 devices: a whole 4x4x8 slice. The times are simulated.
256 devices in a mesh: sp: 32 (over z, x), tp: 8 (over y, core).
Axes of the slice: x: 4, y: 4, z: 8, core: 2. Of those that a mesh axis runs over, the one named last changes fastest.
Arguments:
- tokens: bfloat16 [16384, 2048], P('sp', 'tp'), may hold values from -400 to 400
- lru_in: bfloat16 [2048, 1024], P(None, 'tp'), may hold values from -0.125 to 0.125
- lru_gate_in: bfloat16 [2048, 1024], P(None, 'tp'), may hold values from -0.125 to 0.125
- query_w: bfloat16 [2048, 1024], P(None, 'tp'), may hold values from -1 to 1
- key_w: bfloat16 [2048, 1024], P(None, 'tp'), may hold values from -10 to 10
- value_w: bfloat16 [2048, 1024], P(None, 'tp'), may hold values from -0.125 to 0.125
- conv_weight: bfloat16 [4, 1024], replicated, may hold values from -3 to 3
- recur_gate_w: bfloat16 [16, 64, 64], replicated, may hold values from -0.75 to 0.75
- input_gate_w: bfloat16 [16, 64, 64], replicated, may hold values from -0.75 to 0.75
- rate_param: float32 [1024], replicated, may hold values from 0 to 16
- decay_extra: float32 [16384, 1024], P('sp', 'tp'), may hold values from -2 to 0
- forget_cum: float32 [16384, 8], P('sp', 'tp'), may hold values from -1538 to 0, as said below
- out_lru: bfloat16 [1024, 2048], P('tp'), may hold values from -0.1875 to 0.1875
- out_fox: bfloat16 [1024, 2048], P('tp'), may hold values from -0.1875 to 0.1875
Outputs:
- mixed_out: bfloat16 [16384, 2048], P('sp', 'tp')
Inputs may be any that keep to these rules, and one draw needn't show every extreme that they name: `forget_cum`: non-increasing along positions in every head.
All inputs are finite; a program needn't handle non-finite values.
Results may differ from a plain program's by a relative error of at most 0.014.
Values may be sent and summed in bfloat16 or wider, within the bound.
A program may use at most 64 MiB of HBM per device.

v0:
```python
import math

import jax
import jax.numpy as jnp
from jax import lax
from jax.sharding import PartitionSpec as P

D = 2048
HEAD_DIM = 128


decay_sharpness = 8.0
epsilon_norm = 1e-06


def in_order(tiles, dim):
    dims = list(tiles.shape[1:])
    dims[dim] *= tiles.shape[0]
    return jnp.moveaxis(tiles, 0, dim).reshape(dims)


def sent_to_all(x, axis):
    copies = jnp.broadcast_to(x, (lax.axis_size(axis), *x.shape))
    return lax.all_to_all(copies, axis, split_axis=0, concat_axis=0, tiled=True)


def gather_directly(x, axis, dim):
    return in_order(sent_to_all(x, axis), dim)


def from_behind(block, axis, distance):
    devices = range(lax.axis_size(axis))
    route = [(i - distance, i) for i in devices if i - distance in devices]
    return lax.ppermute(block, axis, route)


def collected_together(x, axis):
    leaves = jax.tree.leaves(x)
    turns = sorted(range(len(leaves)), key=lambda k: -leaves[k].size)
    width = (1, *leaves[turns[0]].shape)[-1]
    lines = [
        jnp.pad(leaves[k].reshape(-1), (0, -leaves[k].size % width)).reshape(-1, width)
        for k in turns
    ]
    both, at, found = (sent_to_all(jnp.concatenate(lines), axis), 0, {})
    for k, line in zip(turns, lines):
        slab = both[:, at : at + len(line)].reshape(len(both), -1)
        found[k] = slab[:, : leaves[k].size].reshape(-1, *leaves[k].shape)
        at += len(line)
    numbers = iter(range(len(leaves)))
    return jax.tree.map(lambda _: found[next(numbers)], x)


def joined_by_halves(pieces, combine):
    while len(jax.tree.leaves(pieces)[0]) > 1:
        pieces = jax.vmap(combine)(
            *(jax.tree.map(lambda part: part[side::2], pieces) for side in (0, 1))
        )
    return jax.tree.map(lambda part: part[0], pieces)


def prefix_2(x, axis, combine, identity):
    devices, mine = (lax.axis_size(axis), lax.axis_index(axis))
    passed = jnp.arange(devices) < mine

    def kept(part, zero, own):
        part = jnp.where(
            passed.reshape(-1, *(1 for _ in own.shape)), part, jnp.asarray(zero, own.dtype)
        )
        return part

    pieces = collected_together(x, axis)
    return joined_by_halves(jax.tree.map(kept, pieces, identity, x), combine)


def sent_together(arrays, axis, dim, along):
    both = jnp.concatenate(arrays, axis=along)
    filled, at, gathered = (lax.all_gather(both, axis, axis=dim, tiled=True), 0, [])
    for a in arrays:
        gathered.append(lax.slice_in_dim(filled, at, at + a.shape[along], axis=along))
        at += a.shape[along]
    return tuple(gathered)


def cut_along(x, dim, devices):
    dims = x.shape
    tiles = x.reshape(*dims[:dim], devices, dims[dim] // devices, *dims[dim + 1 :])
    return jnp.moveaxis(tiles, dim, 0)


def sent_and_summed(x, axis, dim):
    tiles = cut_along(x, dim, lax.axis_size(axis))
    arrived = lax.all_to_all(tiles, axis, split_axis=0, concat_axis=0, tiled=True)
    return arrived.astype(jnp.float32).sum(axis=0)


def combine_pairs(earlier, later):
    decay_one, state_one = earlier
    decay_two, state_two = later
    return (decay_one * decay_two, decay_two * state_one + state_two)


def shards(
    tokens,
    lru_in,
    lru_gate_in,
    query_w,
    key_w,
    value_w,
    conv_weight,
    recur_gate_w,
    input_gate_w,
    rate_param,
    decay_extra,
    forget_cum,
    out_lru,
    out_fox,
):
    tok_rows = tokens.shape[0]
    lru_cols = lru_in.shape[1]
    fox_cols = query_w.shape[1]
    tp_index = lax.axis_index("tp")
    weight_all = jnp.concatenate([lru_in, lru_gate_in, query_w, key_w, value_w], 1)
    portion = gather_directly(tokens, "tp", 1)
    weight_part = weight_all
    portion_f32 = portion.astype(jnp.float32)
    projected = jnp.dot(portion, weight_part, preferred_element_type=jnp.float32)
    squares = jnp.sum(portion_f32 * portion_f32, axis=1)
    row_scale = lax.rsqrt(squares / D + epsilon_norm)
    scaled = (projected * row_scale[:, None]).astype(jnp.bfloat16)
    lru_input = scaled[:, :lru_cols]
    gate_input = scaled[:, lru_cols : 2 * lru_cols]
    queries = scaled[:, 2 * lru_cols : 2 * lru_cols + fox_cols]
    keys_dev = scaled[:, 2 * lru_cols + fox_cols : 2 * lru_cols + 2 * fox_cols]
    values_dev = scaled[:, 2 * lru_cols + 2 * fox_cols :]
    taps = conv_weight.shape[0]
    own_conv = lax.dynamic_slice_in_dim(conv_weight, tp_index * lru_cols, lru_cols, 1)
    earlier_rows = from_behind(lru_input[tok_rows - (taps - 1) :], "sp", 1)
    padded = jnp.concatenate([earlier_rows, lru_input], 0)
    conv_sum = jnp.zeros((tok_rows, lru_cols), jnp.float32)
    for tap_idx in range(taps):
        conv_sum = conv_sum + own_conv[tap_idx].astype(jnp.float32)[None, :] * padded[
            tap_idx : tap_idx + tok_rows
        ].astype(jnp.float32)
    conv_out = conv_sum.astype(jnp.bfloat16)
    block_width = recur_gate_w.shape[1]
    blocks_dev = lru_cols // block_width
    own_recur = lax.dynamic_slice_in_dim(recur_gate_w, tp_index * blocks_dev, blocks_dev, 0)
    own_input = lax.dynamic_slice_in_dim(input_gate_w, tp_index * blocks_dev, blocks_dev, 0)
    blocked = conv_out.reshape(tok_rows, blocks_dev, block_width)
    recur_gate = jax.nn.sigmoid(
        jnp.einsum("tnc,ncd->tnd", blocked, own_recur, preferred_element_type=jnp.float32).reshape(
            tok_rows, lru_cols
        )
    )
    input_gate = jax.nn.sigmoid(
        jnp.einsum("tnc,ncd->tnd", blocked, own_input, preferred_element_type=jnp.float32).reshape(
            tok_rows, lru_cols
        )
    )
    own_rate = lax.dynamic_slice_in_dim(rate_param, tp_index * lru_cols, lru_cols, 0)
    log_decay = -decay_sharpness * jax.nn.softplus(-own_rate)[None, :] * recur_gate + decay_extra
    driven = jnp.sqrt(-jnp.expm1(2.0 * log_decay)) * input_gate * conv_out.astype(jnp.float32)
    prefix, local_states = lax.associative_scan(combine_pairs, (jnp.exp(log_decay), driven), axis=0)
    identity = (jnp.ones((lru_cols,), jnp.float32), jnp.zeros((lru_cols,), jnp.float32))
    incoming = prefix_2(
        (prefix[tok_rows - 1], local_states[tok_rows - 1]), "sp", combine_pairs, identity
    )
    states = local_states + prefix * incoming[1][None, :]
    lru_out = (states * jax.nn.gelu(gate_input.astype(jnp.float32))).astype(jnp.bfloat16)
    heads_dev = fox_cols // HEAD_DIM
    score_scale = HEAD_DIM ** (-0.5)
    gates_all = gather_directly(forget_cum, "sp", 0)
    sp_index = lax.axis_index("sp")
    offset = sp_index * tok_rows
    query_sets = (queries, offset)
    groups = []
    query_rows, query_first = query_sets
    count = query_rows.shape[0]
    query_heads = query_rows.reshape(count, heads_dev, HEAD_DIM)
    query_cum = lax.dynamic_slice_in_dim(gates_all, query_first, count, 0).T
    query_pos = query_first + jnp.arange(count)
    groups.append((query_heads, query_cum, query_pos, query_first + count - 1))

    def key_block(running, group, key_rows, value_rows, key_first):
        query_heads, query_cum, query_pos, last_query = group
        length = key_rows.shape[0]

        def active(current):
            maxima, totals, weighted = current
            key_cum = lax.dynamic_slice_in_dim(gates_all, key_first, length, 0).T
            key_heads = key_rows.reshape(length, heads_dev, HEAD_DIM)
            value_heads = value_rows.reshape(length, heads_dev, HEAD_DIM)
            scores = (
                jnp.einsum(
                    "qhd,khd->hqk", query_heads, key_heads, preferred_element_type=jnp.float32
                )
                * score_scale
            )
            scores = scores + query_cum[:, :, None] - key_cum[:, None, :]
            key_pos = key_first + jnp.arange(length)
            causal = (query_pos[:, None] >= key_pos[None, :])[None]
            scores = jnp.where(causal, scores, -1e30)
            new_maxima = jnp.maximum(maxima, jnp.max(scores, axis=2))
            probs = jnp.where(causal, jnp.exp(scores - new_maxima[:, :, None]), 0.0)
            rescale = jnp.exp(maxima - new_maxima)
            new_totals = totals * rescale + jnp.sum(probs, axis=2)
            new_weighted = weighted * rescale[:, :, None] + jnp.einsum(
                "hqk,khd->hqd",
                probs.astype(jnp.bfloat16),
                value_heads,
                preferred_element_type=jnp.float32,
            )
            return (new_maxima, new_totals, new_weighted)

        def unchanged(current):
            return current

        return lax.cond(key_first <= last_query, active, unchanged, running)

    def visit_all(running, key_rows, value_rows, key_first):
        return tuple(
            (
                key_block(running[slot], groups[slot], key_rows, value_rows, key_first)
                for slot in range(len(groups))
            )
        )

    attn_start = tuple(
        (
            (
                jnp.full((heads_dev, group[0].shape[0]), -1e30, jnp.float32),
                jnp.zeros((heads_dev, group[0].shape[0]), jnp.float32),
                jnp.zeros((heads_dev, group[0].shape[0], HEAD_DIM), jnp.float32),
            )
            for group in groups
        )
    )
    key_rows, value_rows = sent_together((keys_dev, values_dev), "sp", 0, 1)
    length = key_rows.shape[0]
    blk_len = math.gcd(length, 1024)
    block_count = length // blk_len
    key_blocks = key_rows.reshape(block_count, blk_len, key_rows.shape[1])
    value_blocks = value_rows.reshape(block_count, blk_len, value_rows.shape[1])

    def visit_block(current, block_item):
        block_keys, block_values, block_number = block_item
        return (visit_all(current, block_keys, block_values, block_number * blk_len), None)

    result, unused_out = lax.scan(
        visit_block, attn_start, (key_blocks, value_blocks, jnp.arange(block_count))
    )
    results = []
    for maxima, totals, weighted in result:
        count = weighted.shape[1]
        results.append(
            (weighted / totals[:, :, None])
            .transpose(1, 0, 2)
            .reshape(count, fox_cols)
            .astype(jnp.bfloat16)
        )
    fox_out = results[0]
    branch = jnp.concatenate([lru_out, fox_out], 1)
    weight_rows = jnp.concatenate([out_lru, out_fox], 0)
    weight_part = weight_rows
    mixed_out = sent_and_summed(
        lax.dot_general(
            weight_part, branch, (((0,), (1,)), ((), ())), preferred_element_type=jnp.float32
        ).astype(jnp.bfloat16),
        "tp",
        0,
    )
    return mixed_out.T.astype(jnp.bfloat16)


def solution(mesh):
    placed = (
        P("sp", "tp"),
        P(None, "tp"),
        P(None, "tp"),
        P(None, "tp"),
        P(None, "tp"),
        P(None, "tp"),
        P(),
        P(),
        P(),
        P(),
        P("sp", "tp"),
        P("sp", "tp"),
        P("tp", None),
        P("tp", None),
    )
    return jax.shard_map(
        shards, mesh=mesh, in_specs=placed, out_specs=P("sp", "tp"), check_vma=False
    )
```

profile of v0, /device:TPU:228, one launch (start us, length us, event | category | flops | bytes accessed | tf_op | source)
XLA Modules:
  0.0 267.7 jit_solution(14034074125153756458)
XLA Ops:
  6.5 1.1 copy.29
  7.7 1.5 broadcast_in_dim.57
  9.2 4.6 %all-to-all-start = ((bf16[8,512,256]{1,2,0:T(8,128)(2,1)}), bf16[8,512,256]{1,2,0:T(8,128)(2,1)S(1)}, u32[]{:S(2)}, u32[]{:S(2)}) async-start(bf16[8,512,256]{1,2,0:T(8,128)(2,1)} %broadcast_in_dim.57), calls=%async_computation | async-start | bytes 4194304 | tf_op jit(solution)/shard_map/all_to_all | solution.py:24
  16.5 0.9 constant_dynamic-update-slice_fusion.1
  18.3 22.7 %all-to-all-done = bf16[8,512,256]{1,2,0:T(8,128)(2,1)S(1)} async-done(((bf16[8,512,256]{1,2,0:T(8,128)(2,1)}), bf16[8,512,256]{1,2,0:T(8,128)(2,1)S(1)}, u32[]{:S(2)}, u32[]{:S(2)}) %all-to-all-start) | async-done | bytes 2097184 | tf_op jit(solution)/shard_map/all_to_all | solution.py:24
  41.5 3.6 %fusion.18 = bf16[512,640]{1,0:T(8,128)(2,1)S(1)} fusion(bf16[2048,640]{1,0:T(8,128)(2,1)} %constant_dynamic-update-slice_fusion, bf16[512,2048]{0,1:T(8,128)(2,1)S(1)} %bitcast.74, f32[512]{0:T(512)S(1)} %add_rsqrt_fusion), kind=kOutput, calls=%fused_computation.27 | convolution fusion | flops 1342832640 | bytes 5376000 | tf_op jit(solution)/shard_map/dot_general | solution.py:127
  46.5 8.5 %all-to-all-start.2 = ((f32[32,512,1]{1,2,0:T(1,128)}), f32[32,512,1]{1,2,0:T(1,128)S(1)}, u32[]{:S(2)}, u32[]{:S(2)}) async-start(f32[32,512,1]{1,2,0:T(1,128)} %broadcast_in_dim.65), calls=%async_computation.2 | async-start | bytes 131072 | tf_op jit(solution)/shard_map/all_to_all | solution.py:24
  56.5 3.2 %collective-permute-start = (bf16[3,128]{1,0:T(4,128)(2,1)S(1)}, bf16[3,128]{1,0:T(4,128)(2,1)S(1)}, u32[]{:S(2)}, u32[]{:S(2)}) collective-permute-start(bf16[3,128]{1,0:T(4,128)(2,1)S(1)} %slice.495), channel_id=1, source_target_pairs={{0,8},{8,16},{16,24},{24,32},{32,40},{40,48},{48,56},{56,64},{64,7... | collective-permute-start | bytes 2312 | tf_op jit(solution)/shard_map/ppermute | solution.py:34
  59.8 2.3 collective-permute-done
  62.8 1.0 fusion.21
  68.1 10.7 %all-to-all-start.1 = ((f32[32,2,128]{2,1,0:T(2,128)}), f32[32,2,128]{2,1,0:T(2,128)S(1)}, u32[]{:S(2)}, u32[]{:S(2)}) async-start(f32[32,2,128]{2,1,0:T(2,128)} %broadcast_in_dim.59), calls=%async_computation.1 | async-start | bytes 65536 | tf_op jit(solution)/shard_map/all_to_all | solution.py:24
  78.8 5.5 %all-to-all-done.1 = f32[32,2,128]{2,1,0:T(2,128)S(1)} async-done(((f32[32,2,128]{2,1,0:T(2,128)}), f32[32,2,128]{2,1,0:T(2,128)S(1)}, u32[]{:S(2)}, u32[]{:S(2)}) %all-to-all-start.1) | async-done | bytes 32800 | tf_op jit(solution)/shard_map/all_to_all | solution.py:24
  84.9 53.8 %all-gather.2.cloned.1.call-done = bf16[16384,256]{1,0:T(8,128)(2,1)} async-done(((bf16[512,256]{1,0:T(8,128)(2,1)}), bf16[16384,256]{1,0:T(8,128)(2,1)}) %all-gather.2.cloned.1.call-update) | async-done | bytes 8388624 | tf_op jit(solution)/shard_map/all_gather | solution.py:78
  138.7 5.7 %fusion.54 = (bf16[16384,128]{1,0:T(8,128)(2,1)}, bf16[16384,128]{1,0:T(8,128)(2,1)}) fusion(bf16[16384,256]{1,0:T(8,128)(2,1)} %all-gather.2.cloned.1.call-done), kind=kLoop, calls=%fused_computation.145 | loop fusion | bytes 16777216 | tf_op jit(solution)/shard_map/slice | solution.py:80
  144.5 82.9 %while.15 = (s32[]{:T(128)}, f32[1,512]{1,0:T(1,128)S(1)}, f32[1,512]{1,0:T(1,128)S(1)}, f32[1,512,128]{2,1,0:T(8,128)S(1)}, s32[16]{0:T(128)S(1)}, /*index=5*/s...) while((s32[]{:T(128)}, f32[1,512]{1,0:T(1,128)S(1)}, ...), condition=%wide.region_6.7_spmd.clone, body=%wide.region_1.6_spmd.clone.sunk | while | flops 275909120 | bytes 7548273 | solution.py:250
  145.8 3.9 %conditional.3 = ((f32[1,512]{1,0:T(1,128)S(1)}, f32[1,512]{1,0:T(1,128)S(1)}, f32[1,512,128]{2,1,0:T(8,128)S(1)})) conditional(s32[]{:T(128)} %convert_element_type.123, (f32[1,512]{1,0:T(1,128)S(1)}, f32[1,512]{1,0:T(1,128)S(1)}, f32[1,512,128]{2,1,0:T(8,128)S(1)}) %tuple.73, (s32[]{:T(128)}, s32[]{:T(128)}, bf16[16,1024,128]{2,1,0:T(8,128)(2,1)}, ...), branch_computations={%region_2.2_spmd, %region_3.5_spmd} | conditional | flops 275909120 | bytes 7545934 | solution.py:219
  145.9 1.6 fusion.53
  148.0 1.7 fusion.4
  151.0 3.9 %conditional.3 = ((f32[1,512]{1,0:T(1,128)S(1)}, f32[1,512]{1,0:T(1,128)S(1)}, f32[1,512,128]{2,1,0:T(8,128)S(1)})) conditional(s32[]{:T(128)} %convert_element_type.123, (f32[1,512]{1,0:T(1,128)S(1)}, f32[1,512]{1,0:T(1,128)S(1)}, f32[1,512,128]{2,1,0:T(8,128)S(1)}) %tuple.73, (s32[]{:T(128)}, s32[]{:T(128)}, bf16[16,1024,128]{2,1,0:T(8,128)(2,1)}, ...), branch_computations={%region_2.2_spmd, %region_3.5_spmd} | conditional | flops 275909120 | bytes 7545934 | solution.py:219
  151.1 1.6 fusion.53
  153.1 1.7 fusion.4
  156.1 3.9 %conditional.3 = ((f32[1,512]{1,0:T(1,128)S(1)}, f32[1,512]{1,0:T(1,128)S(1)}, f32[1,512,128]{2,1,0:T(8,128)S(1)})) conditional(s32[]{:T(128)} %convert_element_type.123, (f32[1,512]{1,0:T(1,128)S(1)}, f32[1,512]{1,0:T(1,128)S(1)}, f32[1,512,128]{2,1,0:T(8,128)S(1)}) %tuple.73, (s32[]{:T(128)}, s32[]{:T(128)}, bf16[16,1024,128]{2,1,0:T(8,128)(2,1)}, ...), branch_computations={%region_2.2_spmd, %region_3.5_spmd} | conditional | flops 275909120 | bytes 7545934 | solution.py:219
  156.3 1.6 fusion.53
  158.3 1.7 fusion.4
  161.3 3.9 %conditional.3 = ((f32[1,512]{1,0:T(1,128)S(1)}, f32[1,512]{1,0:T(1,128)S(1)}, f32[1,512,128]{2,1,0:T(8,128)S(1)})) conditional(s32[]{:T(128)} %convert_element_type.123, (f32[1,512]{1,0:T(1,128)S(1)}, f32[1,512]{1,0:T(1,128)S(1)}, f32[1,512,128]{2,1,0:T(8,128)S(1)}) %tuple.73, (s32[]{:T(128)}, s32[]{:T(128)}, bf16[16,1024,128]{2,1,0:T(8,128)(2,1)}, ...), branch_computations={%region_2.2_spmd, %region_3.5_spmd} | conditional | flops 275909120 | bytes 7545934 | solution.py:219
  161.4 1.6 fusion.53
  163.5 1.7 fusion.4
  166.5 3.9 %conditional.3 = ((f32[1,512]{1,0:T(1,128)S(1)}, f32[1,512]{1,0:T(1,128)S(1)}, f32[1,512,128]{2,1,0:T(8,128)S(1)})) conditional(s32[]{:T(128)} %convert_element_type.123, (f32[1,512]{1,0:T(1,128)S(1)}, f32[1,512]{1,0:T(1,128)S(1)}, f32[1,512,128]{2,1,0:T(8,128)S(1)}) %tuple.73, (s32[]{:T(128)}, s32[]{:T(128)}, bf16[16,1024,128]{2,1,0:T(8,128)(2,1)}, ...), branch_computations={%region_2.2_spmd, %region_3.5_spmd} | conditional | flops 275909120 | bytes 7545934 | solution.py:219
  166.6 1.6 fusion.53
  168.7 1.7 fusion.4
  171.7 3.9 %conditional.3 = ((f32[1,512]{1,0:T(1,128)S(1)}, f32[1,512]{1,0:T(1,128)S(1)}, f32[1,512,128]{2,1,0:T(8,128)S(1)})) conditional(s32[]{:T(128)} %convert_element_type.123, (f32[1,512]{1,0:T(1,128)S(1)}, f32[1,512]{1,0:T(1,128)S(1)}, f32[1,512,128]{2,1,0:T(8,128)S(1)}) %tuple.73, (s32[]{:T(128)}, s32[]{:T(128)}, bf16[16,1024,128]{2,1,0:T(8,128)(2,1)}, ...), branch_computations={%region_2.2_spmd, %region_3.5_spmd} | conditional | flops 275909120 | bytes 7545934 | solution.py:219
  171.8 1.6 fusion.53
  173.8 1.7 fusion.4
  176.9 3.9 %conditional.3 = ((f32[1,512]{1,0:T(1,128)S(1)}, f32[1,512]{1,0:T(1,128)S(1)}, f32[1,512,128]{2,1,0:T(8,128)S(1)})) conditional(s32[]{:T(128)} %convert_element_type.123, (f32[1,512]{1,0:T(1,128)S(1)}, f32[1,512]{1,0:T(1,128)S(1)}, f32[1,512,128]{2,1,0:T(8,128)S(1)}) %tuple.73, (s32[]{:T(128)}, s32[]{:T(128)}, bf16[16,1024,128]{2,1,0:T(8,128)(2,1)}, ...), branch_computations={%region_2.2_spmd, %region_3.5_spmd} | conditional | flops 275909120 | bytes 7545934 | solution.py:219
  177.0 1.6 fusion.53
  179.0 1.7 fusion.4
  182.0 3.9 %conditional.3 = ((f32[1,512]{1,0:T(1,128)S(1)}, f32[1,512]{1,0:T(1,128)S(1)}, f32[1,512,128]{2,1,0:T(8,128)S(1)})) conditional(s32[]{:T(128)} %convert_element_type.123, (f32[1,512]{1,0:T(1,128)S(1)}, f32[1,512]{1,0:T(1,128)S(1)}, f32[1,512,128]{2,1,0:T(8,128)S(1)}) %tuple.73, (s32[]{:T(128)}, s32[]{:T(128)}, bf16[16,1024,128]{2,1,0:T(8,128)(2,1)}, ...), branch_computations={%region_2.2_spmd, %region_3.5_spmd} | conditional | flops 275909120 | bytes 7545934 | solution.py:219
  182.2 1.6 fusion.53
  184.2 1.7 fusion.4
  187.2 3.9 %conditional.3 = ((f32[1,512]{1,0:T(1,128)S(1)}, f32[1,512]{1,0:T(1,128)S(1)}, f32[1,512,128]{2,1,0:T(8,128)S(1)})) conditional(s32[]{:T(128)} %convert_element_type.123, (f32[1,512]{1,0:T(1,128)S(1)}, f32[1,512]{1,0:T(1,128)S(1)}, f32[1,512,128]{2,1,0:T(8,128)S(1)}) %tuple.73, (s32[]{:T(128)}, s32[]{:T(128)}, bf16[16,1024,128]{2,1,0:T(8,128)(2,1)}, ...), branch_computations={%region_2.2_spmd, %region_3.5_spmd} | conditional | flops 275909120 | bytes 7545934 | solution.py:219
  187.3 1.6 fusion.53
  189.4 1.7 fusion.4
  192.4 3.9 %conditional.3 = ((f32[1,512]{1,0:T(1,128)S(1)}, f32[1,512]{1,0:T(1,128)S(1)}, f32[1,512,128]{2,1,0:T(8,128)S(1)})) conditional(s32[]{:T(128)} %convert_element_type.123, (f32[1,512]{1,0:T(1,128)S(1)}, f32[1,512]{1,0:T(1,128)S(1)}, f32[1,512,128]{2,1,0:T(8,128)S(1)}) %tuple.73, (s32[]{:T(128)}, s32[]{:T(128)}, bf16[16,1024,128]{2,1,0:T(8,128)(2,1)}, ...), branch_computations={%region_2.2_spmd, %region_3.5_spmd} | conditional | flops 275909120 | bytes 7545934 | solution.py:219
  192.5 1.6 fusion.53
  194.6 1.7 fusion.4
  197.6 3.9 %conditional.3 = ((f32[1,512]{1,0:T(1,128)S(1)}, f32[1,512]{1,0:T(1,128)S(1)}, f32[1,512,128]{2,1,0:T(8,128)S(1)})) conditional(s32[]{:T(128)} %convert_element_type.123, (f32[1,512]{1,0:T(1,128)S(1)}, f32[1,512]{1,0:T(1,128)S(1)}, f32[1,512,128]{2,1,0:T(8,128)S(1)}) %tuple.73, (s32[]{:T(128)}, s32[]{:T(128)}, bf16[16,1024,128]{2,1,0:T(8,128)(2,1)}, ...), branch_computations={%region_2.2_spmd, %region_3.5_spmd} | conditional | flops 275909120 | bytes 7545934 | solution.py:219
  197.7 1.6 fusion.53
  199.7 1.7 fusion.4
  202.8 3.9 %conditional.3 = ((f32[1,512]{1,0:T(1,128)S(1)}, f32[1,512]{1,0:T(1,128)S(1)}, f32[1,512,128]{2,1,0:T(8,128)S(1)})) conditional(s32[]{:T(128)} %convert_element_type.123, (f32[1,512]{1,0:T(1,128)S(1)}, f32[1,512]{1,0:T(1,128)S(1)}, f32[1,512,128]{2,1,0:T(8,128)S(1)}) %tuple.73, (s32[]{:T(128)}, s32[]{:T(128)}, bf16[16,1024,128]{2,1,0:T(8,128)(2,1)}, ...), branch_computations={%region_2.2_spmd, %region_3.5_spmd} | conditional | flops 275909120 | bytes 7545934 | solution.py:219
  202.9 1.6 fusion.53
  204.9 1.7 fusion.4
  207.9 3.9 %conditional.3 = ((f32[1,512]{1,0:T(1,128)S(1)}, f32[1,512]{1,0:T(1,128)S(1)}, f32[1,512,128]{2,1,0:T(8,128)S(1)})) conditional(s32[]{:T(128)} %convert_element_type.123, (f32[1,512]{1,0:T(1,128)S(1)}, f32[1,512]{1,0:T(1,128)S(1)}, f32[1,512,128]{2,1,0:T(8,128)S(1)}) %tuple.73, (s32[]{:T(128)}, s32[]{:T(128)}, bf16[16,1024,128]{2,1,0:T(8,128)(2,1)}, ...), branch_computations={%region_2.2_spmd, %region_3.5_spmd} | conditional | flops 275909120 | bytes 7545934 | solution.py:219
  208.0 1.6 fusion.53
  210.1 1.7 fusion.4
  213.1 3.9 %conditional.3 = ((f32[1,512]{1,0:T(1,128)S(1)}, f32[1,512]{1,0:T(1,128)S(1)}, f32[1,512,128]{2,1,0:T(8,128)S(1)})) conditional(s32[]{:T(128)} %convert_element_type.123, (f32[1,512]{1,0:T(1,128)S(1)}, f32[1,512]{1,0:T(1,128)S(1)}, f32[1,512,128]{2,1,0:T(8,128)S(1)}) %tuple.73, (s32[]{:T(128)}, s32[]{:T(128)}, bf16[16,1024,128]{2,1,0:T(8,128)(2,1)}, ...), branch_computations={%region_2.2_spmd, %region_3.5_spmd} | conditional | flops 275909120 | bytes 7545934 | solution.py:219
  213.2 1.6 fusion.53
  215.3 1.7 fusion.4
  218.3 3.9 %conditional.3 = ((f32[1,512]{1,0:T(1,128)S(1)}, f32[1,512]{1,0:T(1,128)S(1)}, f32[1,512,128]{2,1,0:T(8,128)S(1)})) conditional(s32[]{:T(128)} %convert_element_type.123, (f32[1,512]{1,0:T(1,128)S(1)}, f32[1,512]{1,0:T(1,128)S(1)}, f32[1,512,128]{2,1,0:T(8,128)S(1)}) %tuple.73, (s32[]{:T(128)}, s32[]{:T(128)}, bf16[16,1024,128]{2,1,0:T(8,128)(2,1)}, ...), branch_computations={%region_2.2_spmd, %region_3.5_spmd} | conditional | flops 275909120 | bytes 7545934 | solution.py:219
  218.4 1.6 fusion.53
  220.5 1.7 fusion.4
  223.5 3.9 %conditional.3 = ((f32[1,512]{1,0:T(1,128)S(1)}, f32[1,512]{1,0:T(1,128)S(1)}, f32[1,512,128]{2,1,0:T(8,128)S(1)})) conditional(s32[]{:T(128)} %convert_element_type.123, (f32[1,512]{1,0:T(1,128)S(1)}, f32[1,512]{1,0:T(1,128)S(1)}, f32[1,512,128]{2,1,0:T(8,128)S(1)}) %tuple.73, (s32[]{:T(128)}, s32[]{:T(128)}, bf16[16,1024,128]{2,1,0:T(8,128)(2,1)}, ...), branch_computations={%region_2.2_spmd, %region_3.5_spmd} | conditional | flops 275909120 | bytes 7545934 | solution.py:219
  223.6 1.6 fusion.53
  225.6 1.7 fusion.4
  228.3 31.3 %all_to_all.20 = bf16[8,256,512]{2,1,0:T(8,128)(2,1)S(1)} all-to-all(bf16[8,256,512]{2,1,0:T(8,128)(2,1)S(1)} %bitcast.77), channel_id=1, replica_groups=mesh['sp'=32,'tp'=8] {'tp'}, dimensions={0} | all-to-all | bytes 4194304 | tf_op jit(solution)/shard_map/all_to_all | solution.py:93
  (364 shorter events, 32.1 us)
Async XLA Ops:
  6.5 55.8 %copy-start = (bf16[16,64,64]{2,1,0:T(8,128)(2,1)S(1)}, bf16[16,64,64]{2,1,0:T(8,128)(2,1)}, u32[]{:S(2)}) copy-start(bf16[16,64,64]{2,1,0:T(8,128)(2,1)} %param.25) | copy-start | bytes 393220
  9.2 4.7 %copy-start.1 = (bf16[2048,128]{1,0:T(8,128)(2,1)S(1)}, bf16[2048,128]{1,0:T(8,128)(2,1)}, u32[]{:S(2)}) copy-start(bf16[2048,128]{1,0:T(8,128)(2,1)} %param.19) | copy-start | bytes 1572868
  9.2 5.5 %copy-start.2 = (bf16[2048,128]{1,0:T(8,128)(2,1)S(1)}, bf16[2048,128]{1,0:T(8,128)(2,1)}, u32[]{:S(2)}) copy-start(bf16[2048,128]{1,0:T(8,128)(2,1)} %param.20) | copy-start | bytes 1572868
  9.2 31.8 %all-to-all-start = ((bf16[8,512,256]{1,2,0:T(8,128)(2,1)}), bf16[8,512,256]{1,2,0:T(8,128)(2,1)S(1)}, u32[]{:S(2)}, u32[]{:S(2)}) async-start(bf16[8,512,256]{1,2,0:T(8,128)(2,1)} %broadcast_in_dim.57), calls=%async_computation | async-start | bytes 4194304 | tf_op jit(solution)/shard_map/all_to_all | solution.py:24
  13.8 124.9 %all-gather.2.cloned.1.call-start = ((), (), s32[]{:S(2)}) async-start(), calls=%async_computation.4 | async-start | bytes 8650752 | tf_op jit(solution)/shard_map/all_gather | solution.py:78
  13.9 1.7 copy-start.3
  13.9 2.6 copy-start.4
  13.9 3.5 %copy-start.5 = (bf16[2048,128]{1,0:T(8,128)(2,1)S(1)}, bf16[2048,128]{1,0:T(8,128)(2,1)}, u32[]{:S(2)}) copy-start(bf16[2048,128]{1,0:T(8,128)(2,1)} %param.23) | copy-start | bytes 1572868
  41.5 4.3 %copy-start.7 = (f32[512,1]{0,1:T(1,128)S(1)}, f32[512,1]{0,1:T(1,128)}, u32[]{:S(2)}) copy-start(f32[512,1]{0,1:T(1,128)} %param.29) | copy-start | bytes 6148
  46.5 20.9 %all-to-all-start.2 = ((f32[32,512,1]{1,2,0:T(1,128)}), f32[32,512,1]{1,2,0:T(1,128)S(1)}, u32[]{:S(2)}, u32[]{:S(2)}) async-start(f32[32,512,1]{1,2,0:T(1,128)} %broadcast_in_dim.65), calls=%async_computation.2 | async-start | bytes 131072 | tf_op jit(solution)/shard_map/all_to_all | solution.py:24
  56.5 7.5 %copy-start.6 = (f32[512,128]{1,0:T(8,128)S(1)}, f32[512,128]{1,0:T(8,128)}, u32[]{:S(2)}) copy-start(f32[512,128]{1,0:T(8,128)} %param.28) | copy-start | bytes 786436
  56.5 5.6 %collective-permute-start = (bf16[3,128]{1,0:T(4,128)(2,1)S(1)}, bf16[3,128]{1,0:T(4,128)(2,1)S(1)}, u32[]{:S(2)}, u32[]{:S(2)}) collective-permute-start(bf16[3,128]{1,0:T(4,128)(2,1)S(1)} %slice.495), channel_id=1, source_target_pairs={{0,8},{8,16},{16,24},{24,32},{32,40},{40,48},{48,56},{56,64},{64,7... | collective-permute-start | bytes 2312 | tf_op jit(solution)/shard_map/ppermute | solution.py:34
  68.1 16.2 %all-to-all-start.1 = ((f32[32,2,128]{2,1,0:T(2,128)}), f32[32,2,128]{2,1,0:T(2,128)S(1)}, u32[]{:S(2)}, u32[]{:S(2)}) async-start(f32[32,2,128]{2,1,0:T(2,128)} %broadcast_in_dim.59), calls=%async_computation.1 | async-start | bytes 65536 | tf_op jit(solution)/shard_map/all_to_all | solution.py:24
  144.5 83.0 %copy-start.8 = (bf16[128,2048]{1,0:T(8,128)(2,1)S(1)}, bf16[128,2048]{1,0:T(8,128)(2,1)}, u32[]{:S(2)}) copy-start(bf16[128,2048]{1,0:T(8,128)(2,1)} %param.31) | copy-start | bytes 1572868
  144.5 83.0 %copy-start.9 = (bf16[128,2048]{1,0:T(8,128)(2,1)S(1)}, bf16[128,2048]{1,0:T(8,128)(2,1)}, u32[]{:S(2)}) copy-start(bf16[128,2048]{1,0:T(8,128)(2,1)} %param.30) | copy-start | bytes 1572868
Sparse Core Ops, SparseCore 0:
  46.0 92.7 all-gather.1
where the time goes:
time: 269 us; the launch traced here: 268 us
  waiting for transfers between devices  84.4 us (31%)
  matrix products  58.3 us (22%)
  blocking collectives  31.3 us (12%)
  local copies, waits for them, and re-layouts  29.7 us (11%)
  starting transfers between devices  27 us (10%)
  between operations  14.5 us (5%)
  loops' own time  11.8 us (4%)
  other arithmetic  10.6 us (4%)
    all_gather x1, waiting for transfers between devices, sent_together(): lax.all_gather(both, axis, axis=dim, tiled=True)  53.8 us
    all_to_all x1, blocking collectives, sent_and_summed(): lax.all_to_all(tiles, axis, split_axis=0, concat_axis=0, tiled=True)  31.3 us
    all_to_all x3, waiting for transfers between devices, sent_to_all(): return lax.all_to_all(copies, axis, split_axis=0, concat_axis=0, tiled=True)  28.2 us
    dot_general x16, matrix products, active(): jnp.einsum('hqk,khd->hqd', probs.astype(jnp.bfloat16), value_heads, prefe...  27.6 us
    dot_general x16, matrix products, active(): jnp.einsum('qhd,khd->hqk', query_heads, key_heads, preferred_element_type...  25.1 us
    all_to_all x3, starting transfers between devices, sent_to_all(): return lax.all_to_all(copies, axis, split_axis=0, concat_axis=0, tiled=True)  23.8 us
    another operation x1, loops' own time, shards(): lax.scan(visit_block, attn_start, (key_blocks, value_blocks, jnp.arange(b...  11 us
    dynamic_slice x16, local copies, waits for them, and re-layouts, shards(): lax.scan(visit_block, attn_start, (key_blocks, value_blocks, jnp.arange(b...  9.39 us
  transfers between devices with their start and end apart: 5, of which 4 were waited for; matrix products, arithmetic and copies ran while one was open for 5% of the time, Pallas kernels for 0%

commit v1 on v0

--- a/solution.py
+++ b/solution.py
@@ -3,6 +3,8 @@
 import jax
 import jax.numpy as jnp
 from jax import lax
+from jax.experimental import pallas as pl
+from jax.experimental.pallas import tpu as pltpu
 from jax.sharding import PartitionSpec as P
 
 D = 2048
@@ -98,6 +100,246 @@
     decay_one, state_one = earlier
     decay_two, state_two = later
     return (decay_one * decay_two, decay_two * state_one + state_two)
+
+
+MESH = pl.DeviceIdType.MESH
+ZS, XS = 8, 4
+BLK = 512
+KROWS = BLK + 16
+TILE = 256
+LOG2E = 1.4426950408889634
+NEG = -1e30
+
+
+def remote(src, dst, send, recv, **where):
+    return pltpu.make_async_remote_copy(
+        src_ref=src, dst_ref=dst, send_sem=send, recv_sem=recv, device_id=where, device_id_type=MESH
+    )
+
+
+def eye_mask():
+    return lax.broadcasted_iota(jnp.int32, (128, 128), 0) == lax.broadcasted_iota(
+        jnp.int32, (128, 128), 1
+    )
+
+
+def packed_rows(column):
+    eye = eye_mask()
+    return jnp.concatenate(
+        [
+            jnp.sum(jnp.where(eye, column[g * 128 : (g + 1) * 128], 0.0), axis=0, keepdims=True)
+            for g in range(4)
+        ],
+        axis=0,
+    )
+
+
+def unpacked_row(row):
+    return jnp.sum(
+        jnp.where(eye_mask(), jnp.broadcast_to(row, (128, 128)), 0.0), axis=1, keepdims=True
+    )
+
+
+def attention_kernel(
+    q_ref, k_ref, v_ref, f_ref, o_ref,
+    kv, qb, bias, m_ref, l_ref, acc, o_send, st_send, o_recv, st_recv,
+    send_p, recv_p, send_m, recv_m, send_q, recv_q, send_o, recv_o, send_s, recv_s,
+):
+    sp = lax.axis_index("sp")
+    z, x = lax.div(sp, XS), lax.rem(sp, XS)
+    up = lax.rem(z + 1, ZS) * XS + x
+    down = lax.rem(z + ZS - 1, ZS) * XS + x
+
+    def beside(r):
+        return z * XS + lax.rem(x + r, XS)
+
+    barrier = pltpu.get_barrier_semaphore()
+    for other in (up, down, beside(1), beside(2), beside(3)):
+        pl.semaphore_signal(barrier, inc=1, device_id={"sp": other}, device_id_type=MESH)
+    pl.semaphore_wait(barrier, 5)
+
+    kv[0, :BLK, :] = k_ref[...]
+    forget = f_ref[...]
+    high = forget.astype(jnp.bfloat16).astype(jnp.float32)
+    middle = (forget - high).astype(jnp.bfloat16).astype(jnp.float32)
+    low = forget - high - middle
+    kv[0, BLK:KROWS, :] = jnp.concatenate(
+        [high, middle, low, jnp.zeros_like(low)], axis=0
+    ).astype(jnp.bfloat16)
+    kv[0, KROWS:, :] = v_ref[...]
+    own_rows = pl.ds(pl.multiple_of(x * BLK, BLK), BLK)
+    qb[own_rows, :] = q_ref[...]
+
+    keys, vals = pl.ds(0, KROWS), pl.ds(KROWS, BLK)
+    plus = [(0, 1, keys), (0, 1, vals), (1, 2, keys), (1, 2, vals), (2, 3, keys), (2, 3, vals), (3, 7, keys)]
+    minus = [(0, 4, keys), (0, 4, vals), (4, 5, keys), (4, 5, vals), (5, 6, keys), (5, 6, vals), (6, 7, vals)]
+    plus = [
+        remote(kv.at[a, rows], kv.at[b, rows], send_p.at[i], recv_p.at[i], sp=up)
+        for i, (a, b, rows) in enumerate(plus)
+    ]
+    minus = [
+        remote(kv.at[a, rows], kv.at[b, rows], send_m.at[i], recv_m.at[i], sp=down)
+        for i, (a, b, rows) in enumerate(minus)
+    ]
+    query_copies = {
+        r: remote(q_ref, qb.at[own_rows], send_q.at[r], recv_q.at[r], sp=beside(r)) for r in (1, 2, 3)
+    }
+    for i in (0, 1):
+        plus[i].start()
+        minus[i].start()
+    for r in (1, 3, 2):
+        query_copies[r].start()
+
+    m_ref[...] = jnp.full_like(m_ref, NEG)
+    l_ref[...] = jnp.zeros_like(l_ref)
+    acc[...] = jnp.zeros_like(acc)
+
+    def set_bias(slot):
+        parts = kv[slot, BLK:KROWS, :].astype(jnp.float32)
+        whole = parts[0:4] + parts[4:8] + parts[8:12]
+        for g in range(4):
+            bias[slot : slot + 1, g * 128 : (g + 1) * 128] = whole[g : g + 1] * -LOG2E
+
+    scale = HEAD_DIM ** (-0.5) * LOG2E
+
+    def tile(i, slot, masked=None):
+        rows = pl.ds(pl.multiple_of(i * TILE, TILE), TILE)
+        scores = lax.dot_general(
+            qb[rows, :], kv[slot, :BLK, :], (((1,), (1,)), ((), ())), preferred_element_type=jnp.float32
+        )
+        scores = scores * scale + bias[slot : slot + 1, :]
+        if masked is not None:
+            seen = lax.broadcasted_iota(jnp.int32, scores.shape, 0) + masked * TILE
+            scores = jnp.where(seen >= lax.broadcasted_iota(jnp.int32, scores.shape, 1), scores, NEG)
+        old = m_ref[rows, :]
+        new = jnp.maximum(old, jnp.max(scores, axis=1, keepdims=True))
+        rescale = jnp.exp2(old - new)
+        probs = jnp.exp2(scores - jnp.concatenate([new] * (BLK // 128), axis=1))
+        total = l_ref[rows, :] * rescale
+        for g in range(BLK // 128):
+            total = total + probs[:, g * 128 : (g + 1) * 128]
+        l_ref[rows, :] = total
+        m_ref[rows, :] = new
+        acc[rows, :] = acc[rows, :] * rescale + jnp.dot(
+            probs.astype(jnp.bfloat16), kv[slot, KROWS:, :], preferred_element_type=jnp.float32
+        )
+
+    tiles = BLK // TILE
+
+    def visit(slot, first=0, last=XS * tiles):
+        def body(i, carry):
+            tile(i, slot)
+            return carry
+
+        lax.fori_loop(first, last, body, 0)
+
+    set_bias(0)
+    for t in range(tiles):
+        tile(x * tiles + t, 0, masked=t)
+    for r in (1, 3, 2):
+        query_copies[r].wait_recv()
+    visit(0, first=(x + 1) * tiles)
+
+    for d in (1, 2, 3):
+        at = 2 * (d - 1)
+        for i in (at, at + 1):
+            plus[i].wait_recv()
+            if i + 2 < 7:
+                plus[i + 2].start()
+            minus[i].wait_recv()
+            if d < 3:
+                minus[i + 2].start()
+            elif i == at + 1:
+                minus[6].start()
+
+        @pl.when(z >= d)
+        def _():
+            set_bias(d)
+            visit(d)
+
+        @pl.when(z + d >= ZS)
+        def _():
+            set_bias(3 + d)
+            visit(3 + d)
+
+    plus[6].wait_recv()
+    minus[6].wait_recv()
+
+    @pl.when(z >= 4)
+    def _():
+        set_bias(7)
+        visit(7)
+
+    out_copies = {
+        r: (
+            remote(o_send.at[r], o_recv.at[r], send_o.at[r], recv_o.at[r], sp=beside(r)),
+            remote(st_send.at[r], st_recv.at[r], send_s.at[r], recv_s.at[r], sp=beside(r)),
+        )
+        for r in (1, 2, 3)
+    }
+
+    def stats(rows):
+        total = jnp.broadcast_to(jnp.sum(l_ref[rows, :], axis=1, keepdims=True), (BLK, 128))
+        return packed_rows(m_ref[rows, :]), packed_rows(total)
+
+    for r in (2, 1, 3):
+        rows = pl.ds(pl.multiple_of(lax.rem(x + r, XS) * BLK, BLK), BLK)
+        o_send[r] = acc[rows, :].astype(jnp.bfloat16)
+        st_send[r] = jnp.concatenate(stats(rows), axis=0)
+        for copy in out_copies[r]:
+            copy.start()
+
+    tops, sums = [None] * 4, [None] * 4
+    tops[0], sums[0] = stats(own_rows)
+    for r in (1, 3, 2):
+        for copy in out_copies[r]:
+            copy.wait_recv()
+        both = st_recv[r]
+        tops[r], sums[r] = both[0:4], both[4:8]
+    top = jnp.maximum(jnp.maximum(tops[0], tops[1]), jnp.maximum(tops[2], tops[3]))
+    shares = [jnp.exp2(t - top) for t in tops]
+    whole = shares[0] * sums[0] + shares[1] * sums[1] + shares[2] * sums[2] + shares[3] * sums[3]
+    shares = [s / whole for s in shares]
+    for g in range(4):
+        part = pl.ds(g * 128, 128)
+        mine = pl.ds(pl.multiple_of(x * BLK + g * 128, 128), 128)
+        total = unpacked_row(shares[0][g : g + 1]) * acc[mine, :]
+        for r in (1, 2, 3):
+            total = total + unpacked_row(shares[r][g : g + 1]) * o_recv[r, part, :].astype(jnp.float32)
+        o_ref[part, :] = total.astype(jnp.bfloat16)
+
+    for copy in plus + minus + list(query_copies.values()):
+        copy.wait_send()
+    for r in (1, 2, 3):
+        for copy in out_copies[r]:
+            copy.wait_send()
+
+
+def attention(q, k, v, f):
+    vmem = pl.BlockSpec(memory_space=pltpu.VMEM)
+    dma = pltpu.SemaphoreType.DMA
+    return pl.pallas_call(
+        attention_kernel,
+        out_shape=jax.ShapeDtypeStruct((BLK, HEAD_DIM), jnp.bfloat16),
+        in_specs=[vmem] * 4,
+        out_specs=vmem,
+        scratch_shapes=[
+            pltpu.VMEM((ZS, KROWS + BLK, 128), jnp.bfloat16),
+            pltpu.VMEM((XS * BLK, 128), jnp.bfloat16),
+            pltpu.VMEM((ZS, BLK), jnp.float32),
+            pltpu.VMEM((XS * BLK, 128), jnp.float32),
+            pltpu.VMEM((XS * BLK, 128), jnp.float32),
+            pltpu.VMEM((XS * BLK, 128), jnp.float32),
+            pltpu.VMEM((XS, BLK, 128), jnp.bfloat16),
+            pltpu.VMEM((XS, 8, 128), jnp.float32),
+            pltpu.VMEM((XS, BLK, 128), jnp.bfloat16),
+            pltpu.VMEM((XS, 8, 128), jnp.float32),
+            dma((7,)), dma((7,)), dma((7,)), dma((7,)),
+            dma((4,)), dma((4,)), dma((4,)), dma((4,)), dma((4,)), dma((4,)),
+        ],
+        compiler_params=pltpu.CompilerParams(collective_id=1, has_side_effects=True),
+        cost_estimate=pl.CostEstimate(flops=2_000_000_000, bytes_accessed=1_000_000, transcendentals=8_000_000),
+    )(q, k, v, f)
 
 
 def shards(
@@ -168,98 +410,7 @@
     )
     states = local_states + prefix * incoming[1][None, :]
     lru_out = (states * jax.nn.gelu(gate_input.astype(jnp.float32))).astype(jnp.bfloat16)
-    heads_dev = fox_cols // HEAD_DIM
-    score_scale = HEAD_DIM ** (-0.5)
-    gates_all = gather_directly(forget_cum, "sp", 0)
-    sp_index = lax.axis_index("sp")
-    offset = sp_index * tok_rows
-    query_sets = (queries, offset)
-    groups = []
-    query_rows, query_first = query_sets
-    count = query_rows.shape[0]
-    query_heads = query_rows.reshape(count, heads_dev, HEAD_DIM)
-    query_cum = lax.dynamic_slice_in_dim(gates_all, query_first, count, 0).T
-    query_pos = query_first + jnp.arange(count)
-    groups.append((query_heads, query_cum, query_pos, query_first + count - 1))
-
-    def key_block(running, group, key_rows, value_rows, key_first):
-        query_heads, query_cum, query_pos, last_query = group
-        length = key_rows.shape[0]
-
-        def active(current):
-            maxima, totals, weighted = current
-            key_cum = lax.dynamic_slice_in_dim(gates_all, key_first, length, 0).T
-            key_heads = key_rows.reshape(length, heads_dev, HEAD_DIM)
-            value_heads = value_rows.reshape(length, heads_dev, HEAD_DIM)
-            scores = (
-                jnp.einsum(
-                    "qhd,khd->hqk", query_heads, key_heads, preferred_element_type=jnp.float32
-                )
-                * score_scale
-            )
-            scores = scores + query_cum[:, :, None] - key_cum[:, None, :]
-            key_pos = key_first + jnp.arange(length)
-            causal = (query_pos[:, None] >= key_pos[None, :])[None]
-            scores = jnp.where(causal, scores, -1e30)
-            new_maxima = jnp.maximum(maxima, jnp.max(scores, axis=2))
-            probs = jnp.where(causal, jnp.exp(scores - new_maxima[:, :, None]), 0.0)
-            rescale = jnp.exp(maxima - new_maxima)
-            new_totals = totals * rescale + jnp.sum(probs, axis=2)
-            new_weighted = weighted * rescale[:, :, None] + jnp.einsum(
-                "hqk,khd->hqd",
-                probs.astype(jnp.bfloat16),
-                value_heads,
-                preferred_element_type=jnp.float32,
-            )
-            return (new_maxima, new_totals, new_weighted)
-
-        def unchanged(current):
-            return current
-
-        return lax.cond(key_first <= last_query, active, unchanged, running)
-
-    def visit_all(running, key_rows, value_rows, key_first):
-        return tuple(
-            (
-                key_block(running[slot], groups[slot], key_rows, value_rows, key_first)
-                for slot in range(len(groups))
-            )
-        )
-
-    attn_start = tuple(
-        (
-            (
-                jnp.full((heads_dev, group[0].shape[0]), -1e30, jnp.float32),
-                jnp.zeros((heads_dev, group[0].shape[0]), jnp.float32),
-                jnp.zeros((heads_dev, group[0].shape[0], HEAD_DIM), jnp.float32),
-            )
-            for group in groups
-        )
-    )
-    key_rows, value_rows = sent_together((keys_dev, values_dev), "sp", 0, 1)
-    length = key_rows.shape[0]
-    blk_len = math.gcd(length, 1024)
-    block_count = length // blk_len
-    key_blocks = key_rows.reshape(block_count, blk_len, key_rows.shape[1])
-    value_blocks = value_rows.reshape(block_count, blk_len, value_rows.shape[1])
-
-    def visit_block(current, block_item):
-        block_keys, block_values, block_number = block_item
-        return (visit_all(current, block_keys, block_values, block_number * blk_len), None)
-
-    result, unused_out = lax.scan(
-        visit_block, attn_start, (key_blocks, value_blocks, jnp.arange(block_count))
-    )
-    results = []
-    for maxima, totals, weighted in result:
-        count = weighted.shape[1]
-        results.append(
-            (weighted / totals[:, :, None])
-            .transpose(1, 0, 2)
-            .reshape(count, fox_cols)
-            .astype(jnp.bfloat16)
-        )
-    fox_out = results[0]
+    fox_out = attention(queries, keys_dev, values_dev, forget_cum.reshape(4, 128))
     branch = jnp.concatenate([lru_out, fox_out], 1)
     weight_rows = jnp.concatenate([out_lru, out_fox], 0)
     weight_part = weight_rows

time: 269 us -> 141 us (0.52)
  the two profiles are of different devices: /device:TPU:228 before, /device:TPU:193 now
where the time goes in v1:
time: 141 us; the launch traced here: 139 us
  Pallas kernels  41.2 us (29%)
  blocking collectives  36.8 us (26%)
  waiting for transfers between devices  20.8 us (15%)
  starting transfers between devices  15.7 us (11%)
  local copies, waits for them, and re-layouts  13.6 us (10%)
  matrix products  6.56 us (5%)
  other arithmetic  3.87 us (3%)
    pallas_call x1, Pallas kernels, attention(): pl.pallas_call(attention_kernel, out_shape=jax.ShapeDtypeStruct((BLK, HEA...  41.2 us
    all_to_all x1, blocking collectives, sent_and_summed(): lax.all_to_all(tiles, axis, split_axis=0, concat_axis=0, tiled=True)  36.8 us
    all_to_all x2, waiting for transfers between devices, sent_to_all(): return lax.all_to_all(copies, axis, split_axis=0, concat_axis=0, tiled=True)  18.3 us
    all_to_all x2, starting transfers between devices, sent_to_all(): return lax.all_to_all(copies, axis, split_axis=0, concat_axis=0, tiled=True)  12.4 us
    unnamed x25, local copies, waits for them, and re-layouts  5.71 us
    dot_general x1, matrix products, shards(): jnp.dot(portion, weight_part, preferred_element_type=jnp.float32)  3.58 us
    ppermute x1, starting transfers between devices, from_behind(): return lax.ppermute(block, axis, route)  3.25 us
  transfers between devices with their start and end apart: 3, of which 2 were waited for; matrix products, arithmetic and copies ran while one was open for 6% of the time, Pallas kernels for 30%

profile of v1, /device:TPU:193, one launch (start us, length us, event | category | flops | bytes accessed | tf_op | source)
XLA Modules:
  0.0 139.5 jit_solution(7712189464623041602)
XLA Ops:
  0.0 0.0 copy-start
  0.0 1.1 copy.28
  1.1 1.5 %broadcast_in_dim.32 = bf16[8,512,256]{1,2,0:T(8,128)(2,1)} broadcast(bf16[512,256]{0,1:T(8,128)(2,1)S(1)} %copy.28), dimensions={1,2} | broadcast | bytes 2359296 | tf_op jit(solution)/shard_map/broadcast_in_dim | solution.py:25
  2.7 0.0 copy-start.1
  2.7 0.0 copy-start.2
  2.7 5.3 %all-to-all-start = ((bf16[8,512,256]{1,2,0:T(8,128)(2,1)}), bf16[8,512,256]{1,2,0:T(8,128)(2,1)S(1)}, u32[]{:S(2)}, u32[]{:S(2)}) async-start(bf16[8,512,256]{1,2,0:T(8,128)(2,1)} %broadcast_in_dim.32), calls=%async_computation | async-start | bytes 4194304 | tf_op jit(solution)/shard_map/all_to_all | solution.py:26
  7.9 0.0 copy-start.3
  7.9 0.0 copy-start.4
  8.0 0.5 iota_compare_fusion
  8.5 1.3 fusion.33
  9.8 0.7 constant_dynamic-slice_fusion
  10.5 0.0 copy-done.1
  10.5 0.9 constant_dynamic-update-slice_fusion.4
  11.3 0.0 copy-done.2
  11.3 0.9 constant_dynamic-update-slice_fusion.3
  12.3 1.9 %constant_dynamic-update-slice_fusion.2 = bf16[2048,640]{1,0:T(8,128)(2,1)} fusion(bf16[2048,640]{1,0:T(8,128)(2,1)} %constant_dynamic-update-slice_fusion.3, bf16[2048,128]{1,0:T(8,128)(2,1)} %param.17), kind=kLoop, calls=%fused_computation.67 | loop fusion | bytes 1048576
  14.2 0.0 copy-done.3
  14.2 0.8 constant_dynamic-update-slice_fusion.1
  15.0 0.0 copy-done.4
  15.0 0.9 constant_dynamic-update-slice_fusion
  15.9 18.3 %all-to-all-done = bf16[8,512,256]{1,2,0:T(8,128)(2,1)S(1)} async-done(((bf16[8,512,256]{1,2,0:T(8,128)(2,1)}), bf16[8,512,256]{1,2,0:T(8,128)(2,1)S(1)}, u32[]{:S(2)}, u32[]{:S(2)}) %all-to-all-start) | async-done | bytes 2097184 | tf_op jit(solution)/shard_map/all_to_all | solution.py:26
  34.1 0.5 multiply_reduce_fusion
  34.7 3.6 %fusion.1 = bf16[512,640]{1,0:T(8,128)(2,1)S(1)} fusion(bf16[2048,640]{1,0:T(8,128)(2,1)} %constant_dynamic-update-slice_fusion, bf16[512,2048]{0,1:T(8,128)(2,1)S(1)} %bitcast.38, f32[512]{0:T(512)S(1)} %add_rsqrt_fusion), kind=kOutput, calls=%fused_computation.4 | convolution fusion | flops 1342832640 | bytes 5376000 | tf_op jit(solution)/shard_map/dot_general | solution.py:369
  38.3 0.0 copy-start.5
  38.3 0.0 copy-start.7
  38.3 3.3 %collective-permute-start = (bf16[3,128]{1,0:T(4,128)(2,1)S(1)}, bf16[3,128]{1,0:T(4,128)(2,1)S(1)}, u32[]{:S(2)}, u32[]{:S(2)}) collective-permute-start(bf16[3,128]{1,0:T(4,128)(2,1)S(1)} %slice.492), channel_id=1, source_target_pairs={{0,8},{8,16},{16,24},{24,32},{32,40},{40,48},{48,56},{56,64},{64,7... | collective-permute-start | bytes 2312 | tf_op jit(solution)/shard_map/ppermute | solution.py:36
  41.6 0.8 fusion.35
  42.3 2.5 %collective-permute-done = bf16[3,128]{1,0:T(4,128)(2,1)S(1)} collective-permute-done((bf16[3,128]{1,0:T(4,128)(2,1)S(1)}, bf16[3,128]{1,0:T(4,128)(2,1)S(1)}, u32[]{:S(2)}, u32[]{:S(2)}) %collective-permute-start) | collective-permute-done | bytes 800 | tf_op jit(solution)/shard_map/ppermute | solution.py:36
  44.9 0.1 add_convert_fusion
  45.0 0.1 copy.29
  45.1 0.0 copy-done
  45.1 0.3 fusion.4
  45.4 0.1 copy.32
  45.5 1.0 fusion.7
  46.6 0.1 copy.30
  46.7 0.0 copy-done.5
  46.7 0.0 copy-done.7
  46.7 0.2 convert_multiply_fusion.3
  46.9 0.3 slice.447
  47.2 0.1 slice.385
  47.3 0.3 slice.382
  47.6 0.1 slice.383
  47.7 0.1 slice.384
  47.8 0.1 slice.387
  50.2 0.6 broadcast_in_dim.34
  50.8 7.1 %all-to-all-start.1 = ((f32[32,2,128]{2,1,0:T(2,128)}), f32[32,2,128]{2,1,0:T(2,128)S(1)}, u32[]{:S(2)}, u32[]{:S(2)}) async-start(f32[32,2,128]{2,1,0:T(2,128)} %broadcast_in_dim.34), calls=%async_computation.1 | async-start | bytes 65536 | tf_op jit(solution)/shard_map/all_to_all | solution.py:26
  58.0 0.0 copy-start.6
  58.0 0.0 copy-start.8
  58.0 0.0 copy-start.9
  58.0 41.2 %shard_map.136 = bf16[512,128]{1,0:T(8,128)(2,1)} custom-call(bf16[512,128]{1,0:T(8,128)(2,1)} %get-tuple-element.8.q_ref, bf16[512,128]{1,0:T(8,128)(2,1)} %get-tuple-element.7.k_ref, bf16[512,128]{1,0:T(8,128)(2,1)} %get-tuple-element.6.v_ref, f32[4,128]{1,0:T(4,128)} %bitcast.47), custom_call_target="tpu_custom_call" | custom-call | flops 2000000000 | bytes 1000000 | tf_op jit(solution)/shard_map/pallas_call | solution.py:321
  99.2 0.0 all-to-all-done.1
  99.2 0.0 copy-done.6
  99.2 0.1 broadcast_select_fusion.1
  99.6 0.1 fusion.17
  99.8 0.0 copy-done.8
  99.8 0.0 copy-done.9
  99.8 1.7 %convolution_convert_fusion = bf16[2048,512]{1,0:T(8,128)(2,1)S(1)} fusion(bf16[128,2048]{1,0:T(8,128)(2,1)S(1)} %copy-done.8, bf16[128,2048]{1,0:T(8,128)(2,1)S(1)} %copy-done.9, bf16[512,128]{1,0:T(8,128)(2,1)} %shard_map.136, bf16[512,128]{1,0:T(8,128)(2,1)S(1)} %fusion.17), kind=kOutput, calls=%fused_computation.1 | convolution fusion | flops 540540928 | bytes 3407872 | tf_op jit(solution)/shard_map/dot_general | solution.py:418
  101.5 36.8 %all_to_all.15 = bf16[8,256,512]{2,1,0:T(8,128)(2,1)S(1)} all-to-all(bf16[8,256,512]{2,1,0:T(8,128)(2,1)S(1)} %bitcast.39), channel_id=1, replica_groups=mesh['sp'=32,'tp'=8] {'tp'}, dimensions={0} | all-to-all | bytes 4194304 | tf_op jit(solution)/shard_map/all_to_all | solution.py:95
  138.2 0.4 reduce_sum.22
  138.6 0.8 copy.34
  (162 shorter events, 1.9 us)
Async XLA Ops:
  0.0 45.1 %copy-start = (bf16[16,64,64]{2,1,0:T(8,128)(2,1)S(1)}, bf16[16,64,64]{2,1,0:T(8,128)(2,1)}, u32[]{:S(2)}) copy-start(bf16[16,64,64]{2,1,0:T(8,128)(2,1)} %param.22) | copy-start | bytes 393220
  2.7 7.8 %copy-start.1 = (bf16[2048,128]{1,0:T(8,128)(2,1)S(1)}, bf16[2048,128]{1,0:T(8,128)(2,1)}, u32[]{:S(2)}) copy-start(bf16[2048,128]{1,0:T(8,128)(2,1)} %param.15) | copy-start | bytes 1572868
  2.7 8.7 %copy-start.2 = (bf16[2048,128]{1,0:T(8,128)(2,1)S(1)}, bf16[2048,128]{1,0:T(8,128)(2,1)}, u32[]{:S(2)}) copy-start(bf16[2048,128]{1,0:T(8,128)(2,1)} %param.16) | copy-start | bytes 1572868
  2.7 31.5 %all-to-all-start = ((bf16[8,512,256]{1,2,0:T(8,128)(2,1)}), bf16[8,512,256]{1,2,0:T(8,128)(2,1)S(1)}, u32[]{:S(2)}, u32[]{:S(2)}) async-start(bf16[8,512,256]{1,2,0:T(8,128)(2,1)} %broadcast_in_dim.32), calls=%async_computation | async-start | bytes 4194304 | tf_op jit(solution)/shard_map/all_to_all | solution.py:26
  7.9 6.2 %copy-start.3 = (bf16[2048,128]{1,0:T(8,128)(2,1)S(1)}, bf16[2048,128]{1,0:T(8,128)(2,1)}, u32[]{:S(2)}) copy-start(bf16[2048,128]{1,0:T(8,128)(2,1)} %param.18) | copy-start | bytes 1572868
  7.9 7.1 %copy-start.4 = (bf16[2048,128]{1,0:T(8,128)(2,1)S(1)}, bf16[2048,128]{1,0:T(8,128)(2,1)}, u32[]{:S(2)}) copy-start(bf16[2048,128]{1,0:T(8,128)(2,1)} %param.19) | copy-start | bytes 1572868
  38.3 8.4 %copy-start.5 = (f32[512,128]{1,0:T(8,128)S(1)}, f32[512,128]{1,0:T(8,128)}, u32[]{:S(2)}) copy-start(f32[512,128]{1,0:T(8,128)} %param.24) | copy-start | bytes 786436
  38.3 8.4 %copy-start.7 = (f32[128]{0:T(128)S(1)}, f32[128]{0:T(128)}, u32[]{:S(2)}) copy-start(f32[128]{0:T(128)} %fusion.33) | copy-start | bytes 1540
  38.3 6.6 %collective-permute-start = (bf16[3,128]{1,0:T(4,128)(2,1)S(1)}, bf16[3,128]{1,0:T(4,128)(2,1)S(1)}, u32[]{:S(2)}, u32[]{:S(2)}) collective-permute-start(bf16[3,128]{1,0:T(4,128)(2,1)S(1)} %slice.492), channel_id=1, source_target_pairs={{0,8},{8,16},{16,24},{24,32},{32,40},{40,48},{48,56},{56,64},{64,7... | collective-permute-start | bytes 2312 | tf_op jit(solution)/shard_map/ppermute | solution.py:36
  50.8 48.4 %all-to-all-start.1 = ((f32[32,2,128]{2,1,0:T(2,128)}), f32[32,2,128]{2,1,0:T(2,128)S(1)}, u32[]{:S(2)}, u32[]{:S(2)}) async-start(f32[32,2,128]{2,1,0:T(2,128)} %broadcast_in_dim.34), calls=%async_computation.1 | async-start | bytes 65536 | tf_op jit(solution)/shard_map/all_to_all | solution.py:26
  58.0 41.3 %copy-start.6 = (pred[32]{0:T(512)(128)(4,1)S(1)}, pred[32]{0:T(512)(128)(4,1)}, u32[]{:S(2)}) copy-start(pred[32]{0:T(512)(128)(4,1)} %iota_compare_fusion) | copy-start | bytes 100
  58.0 41.8 %copy-start.8 = (bf16[128,2048]{1,0:T(8,128)(2,1)S(1)}, bf16[128,2048]{1,0:T(8,128)(2,1)}, u32[]{:S(2)}) copy-start(bf16[128,2048]{1,0:T(8,128)(2,1)} %param.27) | copy-start | bytes 1572868
  58.0 41.8 %copy-start.9 = (bf16[128,2048]{1,0:T(8,128)(2,1)S(1)}, bf16[128,2048]{1,0:T(8,128)(2,1)}, u32[]{:S(2)}) copy-start(bf16[128,2048]{1,0:T(8,128)(2,1)} %param.26) | copy-start | bytes 1572868

commit v2 on v1

v2 whole, which is shorter than its diff:
```python
import jax
import jax.numpy as jnp
from jax import lax
from jax.experimental import pallas as pl
from jax.experimental.pallas import tpu as pltpu
from jax.sharding import PartitionSpec as P

MESH = pl.DeviceIdType.MESH
D = 2048
HEAD_DIM = 128
SP, TP = 32, 8
ZS, XS, YS = 8, 4, 4
BLK = 512
HALF = BLK // 2
FEAT = D // TP
OUT = D // TP
KROWS = BLK + 16
LOG2E = 1.4426950408889634
NEG = -1e30
COPIES = 112

decay_sharpness = 8.0
epsilon_norm = 1e-06


def eye_mask():
    return lax.broadcasted_iota(jnp.int32, (128, 128), 0) == lax.broadcasted_iota(
        jnp.int32, (128, 128), 1
    )


def packed_rows(column):
    eye = eye_mask()
    return jnp.concatenate(
        [
            jnp.sum(jnp.where(eye, column[g * 128 : (g + 1) * 128], 0.0), axis=0, keepdims=True)
            for g in range(4)
        ],
        axis=0,
    )


def unpacked_row(row):
    return jnp.sum(
        jnp.where(eye_mask(), jnp.broadcast_to(row, (128, 128)), 0.0), axis=1, keepdims=True
    )


def dot(a, b):
    return jnp.dot(a, b, preferred_element_type=jnp.float32)


def log1p_unit(u):
    s = u / (2.0 + u)
    square = s * s
    total = jnp.full_like(s, 1.0 / 19.0)
    for k in range(17, 0, -2):
        total = total * square + 1.0 / k
    return 2.0 * s * total


def minus_expm1(x):
    near = jnp.full_like(x, 1.0 / 362880.0)
    for k in (40320.0, 5040.0, 720.0, 120.0, 24.0, 6.0, 2.0, 1.0):
        near = near * x + 1.0 / k
    return jnp.where(x > -0.5, -near * x, 1.0 - jnp.exp(x))


class Gather:
    def __init__(self, copy, own, slots, up, down, partner):
        first, second = pl.ds(0, HALF), pl.ds(HALF, HALF)
        self.own, self.slots = own, slots

        def send(a, b, rows, to):
            source = own if a is None else slots.at[a]
            return copy(source.at[rows], slots.at[b, rows], tp=to)

        self.copies = [
            send(None, 0, pl.ds(0, BLK), partner),
            send(None, 1, first, up),
            send(None, 1, second, up),
            send(None, 2, second, down),
            send(None, 2, first, down),
            send(1, 3, first, up),
            send(2, 3, second, down),
            send(1, 4, first, partner),
            send(1, 4, second, partner),
            send(2, 5, first, partner),
            send(2, 5, second, partner),
            send(3, 6, first, partner),
            send(3, 6, second, partner),
        ]

    def start(self, *which):
        for i in which:
            self.copies[i].start()

    def arrived(self, *which):
        for i in which:
            self.copies[i].wait_recv()

    def begin(self):
        self.start(1, 3, 0, 2, 4)

    def relay(self):
        self.arrived(1)
        self.start(5, 7)
        self.arrived(3)
        self.start(6, 10)
        self.arrived(2)
        self.start(8)
        self.arrived(4)
        self.start(9)

    def relay_last(self):
        self.arrived(5)
        self.start(11)
        self.arrived(6)
        self.start(12)

    def finish(self):
        for copy in self.copies:
            copy.wait_send()


def layer_kernel(
    tok_ref, lru_w_hbm, gate_w_hbm, query_w_hbm, key_w_hbm, value_w_hbm,
    conv_ref, recur_ref, input_ref, rate_ref, extra_ref, f_ref, out_lru_ref, out_fox_ref,
    o_ref,
    weights, tokg, acc_kv, acc_rest, squares,
    kv, qb, bias, m_ref, l_ref, acc, o_send, st_send, o_recv, st_recv,
    lru_own, halo, gate_own, decays, drives, row_tiles, col_tiles,
    lru_out, lru_g, fox_out, fox_g, w_out, acc_out,
    send_sems, recv_sems, load_sems,
):
    sp, tp = lax.axis_index("sp"), lax.axis_index("tp")
    z, x = lax.div(sp, XS), lax.rem(sp, XS)
    y, c = lax.div(tp, 2), lax.rem(tp, 2)
    above = lax.rem(z + 1, ZS) * XS + x
    below = lax.rem(z + ZS - 1, ZS) * XS + x
    partner = y * 2 + 1 - c

    def along_y(r, core):
        return lax.rem(y + r, YS) * 2 + core

    def along_x(r):
        return z * XS + lax.rem(x + r, XS)

    def along_z(r):
        return lax.rem(z + r, ZS) * XS + x

    following, preceding = lax.rem(sp + 1, SP), lax.rem(sp + SP - 1, SP)
    used = [0]

    def copy(src, dst, **where):
        i = used[0]
        used[0] += 1
        return pltpu.make_async_remote_copy(
            src_ref=src, dst_ref=dst, send_sem=send_sems.at[i], recv_sem=recv_sems.at[i],
            device_id=where, device_id_type=MESH,
        )

    loads = [
        pltpu.make_async_copy(w, weights.at[i], load_sems.at[i])
        for i, w in enumerate((key_w_hbm, value_w_hbm, query_w_hbm, lru_w_hbm, gate_w_hbm))
    ]
    for load in loads:
        load.start()

    barrier = pltpu.get_barrier_semaphore()
    for r in range(1, TP):
        pl.semaphore_signal(
            barrier, inc=1, device_id={"tp": lax.rem(tp + r, TP)}, device_id_type=MESH
        )
    others = [along_x(r) for r in range(1, XS)] + [along_z(r) for r in range(1, ZS)]
    for other in others + [following, preceding]:
        pl.semaphore_signal(barrier, inc=1, device_id={"sp": other}, device_id_type=MESH)
    pl.semaphore_wait(barrier, TP - 1 + XS - 1 + ZS - 1 + 2)

    tokens = Gather(copy, tok_ref, tokg, along_y(1, c), along_y(3, c), partner)
    tokens.begin()

    def features(r, core):
        return pl.ds(pl.multiple_of(along_y(r, core) * FEAT, FEAT), FEAT)

    def project(block, other, r, group, target, first=False):
        rows = [features(r, c), features(r, 1 - c)]
        right = jnp.concatenate(
            [jnp.concatenate([weights[i, part, :] for part in rows], axis=0) for i in group], axis=1
        )
        product = dot(jnp.concatenate([block[...], other[...]], axis=1), right)
        target[...] = product if first else target[...] + product

    def count_squares(block, other, first=False):
        total = jnp.zeros_like(squares) if first else squares[...]
        for piece in (block, other):
            for g in range(FEAT // 128):
                value = piece[:, g * 128 : (g + 1) * 128].astype(jnp.float32)
                total = total + value * value
        squares[...] = total

    for load in loads:
        load.wait()
    tokens.arrived(0)
    own_pair = (tok_ref, tokg.at[0])
    project(*own_pair, 0, (0, 1), acc_kv, first=True)
    project(*own_pair, 0, (2, 3, 4), acc_rest, first=True)
    count_squares(*own_pair, first=True)
    tokens.relay()
    up_pair, down_pair, far_pair = [(tokg.at[a], tokg.at[a + 3]) for a in (1, 2, 3)]
    tokens.arrived(7, 8)
    project(*up_pair, 3, (0, 1), acc_kv)
    project(*up_pair, 3, (2, 3, 4), acc_rest)
    count_squares(*up_pair)
    tokens.arrived(9, 10)
    project(*down_pair, 1, (0, 1), acc_kv)
    project(*down_pair, 1, (2, 3, 4), acc_rest)
    count_squares(*down_pair)
    tokens.relay_last()
    tokens.arrived(11, 12)
    count_squares(*far_pair)
    row_scale = lax.rsqrt(
        jnp.sum(squares[...], axis=1, keepdims=True) * (1.0 / D) + epsilon_norm
    )
    project(*far_pair, 2, (0, 1), acc_kv)
    keys_values = (acc_kv[...] * row_scale).astype(jnp.bfloat16)
    kv[0, :BLK, :] = keys_values[:, :128]
    kv[0, KROWS:, :] = keys_values[:, 128:]
    forget = f_ref[...]
    high = forget.astype(jnp.bfloat16).astype(jnp.float32)
    middle = (forget - high).astype(jnp.bfloat16).astype(jnp.float32)
    low = forget - high - middle
    kv[0, BLK:KROWS, :] = jnp.concatenate(
        [high, middle, low, jnp.zeros_like(low)], axis=0
    ).astype(jnp.bfloat16)

    keys, vals = pl.ds(0, KROWS), pl.ds(KROWS, BLK)
    plus = [(0, 1, keys), (0, 1, vals), (1, 2, keys), (1, 2, vals), (2, 3, keys), (2, 3, vals), (3, 7, keys)]
    minus = [(0, 4, keys), (0, 4, vals), (4, 5, keys), (4, 5, vals), (5, 6, keys), (5, 6, vals), (6, 7, vals)]
    plus = [copy(kv.at[a, rows], kv.at[b, rows], sp=above) for a, b, rows in plus]
    minus = [copy(kv.at[a, rows], kv.at[b, rows], sp=below) for a, b, rows in minus]
    for i in (0, 1):
        plus[i].start()
        minus[i].start()

    project(*far_pair, 2, (2, 3, 4), acc_rest)
    rest = (acc_rest[...] * row_scale).astype(jnp.bfloat16)
    own_rows = pl.ds(pl.multiple_of(x * BLK, BLK), BLK)
    qb[own_rows, :] = rest[:, :128]
    lru_own[...] = rest[:, 128:256]
    gate_own[...] = rest[:, 256:]
    query_copies = {r: copy(qb.at[own_rows], qb.at[own_rows], sp=along_x(r)) for r in (1, 2, 3)}
    for r in (1, 3, 2):
        query_copies[r].start()
    tail = copy(lru_own.at[pl.ds(BLK - 16, 16)], halo, sp=following)
    tail.start()

    weight_copies = []
    for r in range(1, TP):
        to = lax.rem(tp + r, TP)
        columns = pl.ds(pl.multiple_of(to * OUT, OUT), OUT)
        for k, ref in enumerate((out_lru_ref, out_fox_ref)):
            weight_copies.append(copy(ref.at[:, columns], w_out.at[k, tp], tp=to))
    for each in weight_copies:
        each.start()
    own_columns = pl.ds(pl.multiple_of(tp * OUT, OUT), OUT)
    for k, ref in enumerate((out_lru_ref, out_fox_ref)):
        w_out[k, tp] = ref[:, own_columns]

    m_ref[...] = jnp.full_like(m_ref, NEG)
    l_ref[...] = jnp.zeros_like(l_ref)
    acc[...] = jnp.zeros_like(acc)

    def set_bias(slot):
        parts = kv[slot, BLK:KROWS, :].astype(jnp.float32)
        whole = parts[0:4] + parts[4:8] + parts[8:12]
        for g in range(4):
            bias[slot : slot + 1, g * 128 : (g + 1) * 128] = whole[g : g + 1] * -LOG2E

    scale = HEAD_DIM ** (-0.5) * LOG2E

    def attend(i, slot, masked=False):
        rows = pl.ds(pl.multiple_of(i * BLK, BLK), BLK)
        scores = lax.dot_general(
            qb[rows, :], kv[slot, :BLK, :], (((1,), (1,)), ((), ())), preferred_element_type=jnp.float32
        )
        scores = scores * scale + bias[slot : slot + 1, :]
        if masked:
            earlier = lax.broadcasted_iota(jnp.int32, scores.shape, 0) >= lax.broadcasted_iota(
                jnp.int32, scores.shape, 1
            )
            scores = jnp.where(earlier, scores, NEG)
        old = m_ref[rows, :]
        new = jnp.maximum(old, jnp.max(scores, axis=1, keepdims=True))
        rescale = jnp.exp2(old - new)
        probs = jnp.exp2(scores - jnp.concatenate([new] * (BLK // 128), axis=1))
        total = l_ref[rows, :] * rescale
        for g in range(BLK // 128):
            total = total + probs[:, g * 128 : (g + 1) * 128]
        l_ref[rows, :] = total
        m_ref[rows, :] = new
        acc[rows, :] = acc[rows, :] * rescale + dot(probs.astype(jnp.bfloat16), kv[slot, KROWS:, :])

    def visit(slot, first=0):
        def body(i, carry):
            attend(i, slot)
            return carry

        lax.fori_loop(first, XS, body, 0)

    set_bias(0)
    attend(x, 0, masked=True)

    tail.wait_recv()
    lru_input = lru_own[...].astype(jnp.float32)
    before = halo[8:16, :].astype(jnp.float32) * jnp.where(sp > 0, 1.0, 0.0)
    joined = jnp.concatenate([before, lru_input], axis=0)
    channels = pl.ds(pl.multiple_of(tp * 128, 128), 128)
    taps = conv_ref[:, channels].astype(jnp.float32)
    conv = jnp.zeros((BLK, 128), jnp.float32)
    for j in range(4):
        shifted = joined if j == 3 else pltpu.roll(joined, 3 - j, 0)
        conv = conv + taps[j : j + 1, :] * shifted[8:, :]
    conv = conv.astype(jnp.bfloat16)
    column = lax.broadcasted_iota(jnp.int32, (64, 128), 1)
    row = lax.broadcasted_iota(jnp.int32, (64, 128), 0)
    left = jnp.where(column == row, 1.0, 0.0).astype(jnp.bfloat16)
    right = jnp.where(column == row + 64, 1.0, 0.0).astype(jnp.bfloat16)

    def block_diagonal(ref):
        return jnp.concatenate([dot(ref[2 * tp], left), dot(ref[2 * tp + 1], right)], axis=0)

    gates_w = jnp.concatenate([block_diagonal(recur_ref), block_diagonal(input_ref)], axis=1)
    gates = dot(conv, gates_w.astype(jnp.bfloat16))
    gates = 1.0 / (1.0 + jnp.exp(-gates))
    rate = log1p_unit(jnp.exp(-rate_ref[pl.ds(tp, 1), :]))
    log_decay = (-decay_sharpness * rate) * gates[:, :128] + extra_ref[...]
    drive = jnp.sqrt(minus_expm1(2.0 * log_decay)) * gates[:, 128:] * conv.astype(jnp.float32)
    decay = jnp.exp(log_decay)
    place = lax.broadcasted_iota(jnp.int32, (BLK, 128), 0)
    step = 1
    while step < BLK:
        if step < 8:
            inside = place >= step
            decay_back = jnp.where(inside, pltpu.roll(decay, step, 0), 1.0)
            drive_back = jnp.where(inside, pltpu.roll(drive, step, 0), 0.0)
        else:
            decay_back = jnp.concatenate([jnp.ones((step, 128), jnp.float32), decay[:-step]], axis=0)
            drive_back = jnp.concatenate([jnp.zeros((step, 128), jnp.float32), drive[:-step]], axis=0)
        drive = decay * drive_back + drive
        decay = decay * decay_back
        step *= 2
    decays[...] = decay
    drives[...] = drive

    def tile_of(a, b):
        return jnp.concatenate([a, b, jnp.zeros((6, 128), jnp.float32)], axis=0)

    row_tiles[0] = tile_of(decays[BLK - 1 :, :], drives[BLK - 1 :, :])
    row_copies = {r: copy(row_tiles.at[0], row_tiles.at[r], sp=along_x(r)) for r in (1, 2, 3)}
    for r in (1, 3, 2):
        row_copies[r].start()

    for r in (1, 3, 2):
        query_copies[r].wait_recv()
    visit(0, first=x + 1)

    column_copies = {r: copy(col_tiles.at[0], col_tiles.at[r], sp=along_z(r)) for r in range(1, ZS)}
    branch = Gather(copy, lru_out, lru_g, along_y(1, c), along_y(3, c), partner)
    one, zero = jnp.ones((1, 128), jnp.float32), jnp.zeros((1, 128), jnp.float32)

    def total_of_row():
        for r in (1, 3, 2):
            row_copies[r].wait_recv()
        whole_decay, whole_state, state = one, zero, zero
        for k in range(XS):
            block = row_tiles[lax.rem(x + XS - k, XS)]
            a, b = block[0:1], block[1:2]
            state = jnp.where(k < x, a * state + b, state)
            whole_state = a * whole_state + b
            whole_decay = whole_decay * a
        col_tiles[0] = tile_of(whole_decay, whole_state)
        for r in range(1, ZS):
            column_copies[r].start()

    def recurrence_out():
        for r in range(1, ZS):
            column_copies[r].wait_recv()
        state = zero
        for k in range(ZS):
            block = col_tiles[lax.rem(z + ZS - k, ZS)]
            state = jnp.where(k < z, block[0:1] * state + block[1:2], state)
        for k in range(XS):
            block = row_tiles[lax.rem(x + XS - k, XS)]
            state = jnp.where(k < x, block[0:1] * state + block[1:2], state)
        gate = gate_own[...].astype(jnp.float32)
        inner = 0.7978845608028654 * (gate + 0.044715 * gate * gate * gate)
        gelu = 0.5 * gate * (1.0 + jnp.tanh(inner))
        lru_out[...] = ((drives[...] + decays[...] * state) * gelu).astype(jnp.bfloat16)
        branch.begin()

    beside_attention = {1: total_of_row, 2: recurrence_out, 3: branch.relay}
    for d in (1, 2, 3):
        at = 2 * (d - 1)
        for i in (at, at + 1):
            plus[i].wait_recv()
            if i + 2 < 7:
                plus[i + 2].start()
            minus[i].wait_recv()
            if d < 3:
                minus[i + 2].start()
            elif i == at + 1:
                minus[6].start()

        @pl.when(z >= d)
        def _():
            set_bias(d)
            visit(d)

        @pl.when(z + d >= ZS)
        def _():
            set_bias(3 + d)
            visit(3 + d)

        beside_attention[d]()

    plus[6].wait_recv()
    minus[6].wait_recv()

    @pl.when(z >= 4)
    def _():
        set_bias(7)
        visit(7)

    out_copies = {
        r: (
            copy(o_send.at[r], o_recv.at[r], sp=along_x(r)),
            copy(st_send.at[r], st_recv.at[r], sp=along_x(r)),
        )
        for r in (1, 2, 3)
    }

    def stats(rows):
        total = jnp.broadcast_to(jnp.sum(l_ref[rows, :], axis=1, keepdims=True), (BLK, 128))
        return packed_rows(m_ref[rows, :]), packed_rows(total)

    for r in (2, 1, 3):
        rows = pl.ds(pl.multiple_of(lax.rem(x + r, XS) * BLK, BLK), BLK)
        o_send[r] = acc[rows, :].astype(jnp.bfloat16)
        st_send[r] = jnp.concatenate(stats(rows), axis=0)
        for each in out_copies[r]:
            each.start()

    branch.relay_last()

    def out_weights(k, r, core):
        return w_out[k, along_y(r, core)]

    sources = [(0, c), (0, 1 - c), (3, c), (3, 1 - c), (1, c), (1, 1 - c), (2, c), (2, 1 - c)]

    def branch_product(k, own, slots, which):
        lookup = [None, 0, 1, 4, 2, 5, 3, 6]
        blocks = [own[...] if lookup[i] is None else slots[lookup[i]] for i in which]
        rights = [out_weights(k, *sources[i]) for i in which]
        return dot(jnp.concatenate(blocks, axis=1), jnp.concatenate(rights, axis=0))

    for each in weight_copies:
        each.wait_recv()
    branch.arrived(0, 7, 8, 9, 10, 11, 12)
    acc_out[...] = branch_product(0, lru_out, lru_g, range(8))

    tops, sums = [None] * 4, [None] * 4
    tops[0], sums[0] = stats(own_rows)
    for r in (1, 3, 2):
        for each in out_copies[r]:
            each.wait_recv()
        both = st_recv[r]
        tops[r], sums[r] = both[0:4], both[4:8]
    top = jnp.maximum(jnp.maximum(tops[0], tops[1]), jnp.maximum(tops[2], tops[3]))
    shares = [jnp.exp2(t - top) for t in tops]
    whole = shares[0] * sums[0] + shares[1] * sums[1] + shares[2] * sums[2] + shares[3] * sums[3]
    shares = [s / whole for s in shares]
    for g in range(4):
        part = pl.ds(g * 128, 128)
        mine = pl.ds(pl.multiple_of(x * BLK + g * 128, 128), 128)
        total = unpacked_row(shares[0][g : g + 1]) * acc[mine, :]
        for r in (1, 2, 3):
            total = total + unpacked_row(shares[r][g : g + 1]) * o_recv[r, part, :].astype(jnp.float32)
        fox_out[part, :] = total.astype(jnp.bfloat16)

    heads = Gather(copy, fox_out, fox_g, along_y(1, c), along_y(3, c), partner)
    heads.begin()
    heads.arrived(0)
    acc_out[...] += branch_product(1, fox_out, fox_g, (0, 1))
    heads.relay()
    heads.arrived(7, 8, 9, 10)
    acc_out[...] += branch_product(1, fox_out, fox_g, (2, 3, 4, 5))
    heads.relay_last()
    heads.arrived(11, 12)
    o_ref[...] = (acc_out[...] + branch_product(1, fox_out, fox_g, (6, 7))).astype(jnp.bfloat16)

    for each in plus + minus + [tail] + weight_copies:
        each.wait_send()
    for group in (query_copies, row_copies, column_copies):
        for each in group.values():
            each.wait_send()
    for pair in out_copies.values():
        for each in pair:
            each.wait_send()
    for group in (tokens, branch, heads):
        group.finish()


def layer(
    tokens, lru_in, lru_gate_in, query_w, key_w, value_w, conv_weight, recur_gate_w, input_gate_w,
    rate_param, decay_extra, forget_cum, out_lru, out_fox,
):
    vmem = pl.BlockSpec(memory_space=pltpu.VMEM)
    hbm = pl.BlockSpec(memory_space=pl.ANY)
    bf16, f32 = jnp.bfloat16, jnp.float32
    return pl.pallas_call(
        layer_kernel,
        out_shape=jax.ShapeDtypeStruct((BLK, OUT), bf16),
        in_specs=[vmem] + [hbm] * 5 + [vmem] * 8,
        out_specs=vmem,
        scratch_shapes=[
            pltpu.VMEM((5, D, 128), bf16),
            pltpu.VMEM((7, BLK, FEAT), bf16),
            pltpu.VMEM((BLK, 256), f32),
            pltpu.VMEM((BLK, 384), f32),
            pltpu.VMEM((BLK, 128), f32),
            pltpu.VMEM((ZS, KROWS + BLK, 128), bf16),
            pltpu.VMEM((XS * BLK, 128), bf16),
            pltpu.VMEM((ZS, BLK), f32),
            pltpu.VMEM((XS * BLK, 128), f32),
            pltpu.VMEM((XS * BLK, 128), f32),
            pltpu.VMEM((XS * BLK, 128), f32),
            pltpu.VMEM((XS, BLK, 128), bf16),
            pltpu.VMEM((XS, 8, 128), f32),
            pltpu.VMEM((XS, BLK, 128), bf16),
            pltpu.VMEM((XS, 8, 128), f32),
            pltpu.VMEM((BLK, 128), bf16),
            pltpu.VMEM((16, 128), bf16),
            pltpu.VMEM((BLK, 128), bf16),
            pltpu.VMEM((BLK, 128), f32),
            pltpu.VMEM((BLK, 128), f32),
            pltpu.VMEM((XS, 8, 128), f32),
            pltpu.VMEM((ZS, 8, 128), f32),
            pltpu.VMEM((BLK, 128), bf16),
            pltpu.VMEM((7, BLK, 128), bf16),
            pltpu.VMEM((BLK, 128), bf16),
            pltpu.VMEM((7, BLK, 128), bf16),
            pltpu.VMEM((2, TP, 128, OUT), bf16),
            pltpu.VMEM((BLK, OUT), f32),
            pltpu.SemaphoreType.DMA((COPIES,)),
            pltpu.SemaphoreType.DMA((COPIES,)),
            pltpu.SemaphoreType.DMA((5,)),
        ],
        compiler_params=pltpu.CompilerParams(collective_id=1, has_side_effects=True),
        cost_estimate=pl.CostEstimate(flops=5_000_000_000, bytes_accessed=8_000_000, transcendentals=9_000_000),
    )(
        tokens, lru_in, lru_gate_in, query_w, key_w, value_w, conv_weight, recur_gate_w, input_gate_w,
        rate_param.reshape(TP, 128), decay_extra, forget_cum.reshape(4, 128), out_lru, out_fox,
    )


def solution(mesh):
    placed = (
        P("sp", "tp"),
        P(None, "tp"),
        P(None, "tp"),
        P(None, "tp"),
        P(None, "tp"),
        P(None, "tp"),
        P(),
        P(),
        P(),
        P(),
        P("sp", "tp"),
        P("sp", "tp"),
        P("tp", None),
        P("tp", None),
    )
    return jax.shard_map(
        layer, mesh=mesh, in_specs=placed, out_specs=P("sp", "tp"), check_vma=False
    )
```

time: 141 us -> 72.4 us (0.51)
  the two profiles are of different devices: /device:TPU:193 before, /device:TPU:11 now
where the time goes in v2:
time: 72.4 us; the launch traced here: 72.2 us
  Pallas kernels  70.6 us (98%)
  local copies, waits for them, and re-layouts  1.67 us (2%)
    pallas_call x1, Pallas kernels, layer(): pl.pallas_call(layer_kernel, out_shape=jax.ShapeDtypeStruct((BLK, OUT), b...  70.6 us
    unnamed x1, local copies, waits for them, and re-layouts  1.67 us

profile of v2, /device:TPU:11, one launch (start us, length us, event | category | flops | bytes accessed | tf_op | source)
XLA Modules:
  0.0 72.2 jit_solution(15635682294729792050)
XLA Ops:
  0.0 70.6 %shard_map.136 = bf16[512,256]{1,0:T(8,128)(2,1)} custom-call(bf16[512,256]{1,0:T(8,128)(2,1)} %tok_ref.1, bf16[2048,128]{1,0:T(8,128)(2,1)} %lru_w_hbm.1, bf16[2048,128]{1,0:T(8,128)(2,1)} %gate_w_hbm.1, bf16[2048,128]{1,0:T(8,128)(2,1)} %query_w_hbm.1, bf16[2048,128]{1,0:T(8,128)(2,1)} %key_w_hbm.1, bf16[2048,128]{1,0:T(8,128)(2,1)} %value_w_hbm.1, ...), custom_call_target="tpu_custom_call" | custom-call | flops 5000000000 | bytes 8000000 | tf_op jit(solution)/shard_map/pallas_call | solution.py:521
  70.6 1.7 %copy.16 = bf16[512,256]{1,0:T(8,128)(2,1)} copy(bf16[512,256]{1,0:T(8,128)(2,1)} %shard_map.136) | data formatting | bytes 524288

commit v3 on v2

v3 whole, which is shorter than its diff:
```python
import jax
import jax.numpy as jnp
from jax import lax
from jax.experimental import pallas as pl
from jax.experimental.pallas import tpu as pltpu
from jax.sharding import PartitionSpec as P

MESH = pl.DeviceIdType.MESH
D = 2048
HEAD_DIM = 128
SP, TP = 32, 8
ZS, XS, YS = 8, 4, 4
BLK = 512
HALF = BLK // 2
FEAT = D // TP
OUT = D // TP
HROWS = HALF + 16
PIECE = HROWS + HALF
LOG2E = 1.4426950408889634
NEG = -1e30
COPIES = 152

decay_sharpness = 8.0
epsilon_norm = 1e-06


def eye_mask():
    return lax.broadcasted_iota(jnp.int32, (128, 128), 0) == lax.broadcasted_iota(
        jnp.int32, (128, 128), 1
    )


def packed_rows(column):
    eye = eye_mask()
    return jnp.concatenate(
        [
            jnp.sum(jnp.where(eye, column[g * 128 : (g + 1) * 128], 0.0), axis=0, keepdims=True)
            for g in range(4)
        ],
        axis=0,
    )


def unpacked_row(row):
    return jnp.sum(
        jnp.where(eye_mask(), jnp.broadcast_to(row, (128, 128)), 0.0), axis=1, keepdims=True
    )


def dot(a, b):
    return jnp.dot(a, b, preferred_element_type=jnp.float32)


def log1p_unit(u):
    s = u / (2.0 + u)
    square = s * s
    total = jnp.full_like(s, 1.0 / 19.0)
    for k in range(17, 0, -2):
        total = total * square + 1.0 / k
    return 2.0 * s * total


def minus_expm1(x):
    near = jnp.full_like(x, 1.0 / 362880.0)
    for k in (40320.0, 5040.0, 720.0, 120.0, 24.0, 6.0, 2.0, 1.0):
        near = near * x + 1.0 / k
    return jnp.where(x > -0.5, -near * x, 1.0 - jnp.exp(x))


class Gather:
    def __init__(self, copy, own, slots, up, down, partner, start=0, rows=BLK):
        half = rows // 2
        first, second = pl.ds(start, half), pl.ds(start + half, half)

        def send(a, b, part, to):
            source = own if a is None else slots.at[a]
            return copy(source.at[part], slots.at[b, part], tp=to)

        self.copies = [
            send(None, 0, pl.ds(start, rows), partner),
            send(None, 1, first, up),
            send(None, 1, second, up),
            send(None, 2, second, down),
            send(None, 2, first, down),
            send(1, 3, first, up),
            send(2, 3, second, down),
            send(1, 4, first, partner),
            send(1, 4, second, partner),
            send(2, 5, first, partner),
            send(2, 5, second, partner),
            send(3, 6, first, partner),
            send(3, 6, second, partner),
        ]

    def start(self, *which):
        for i in which:
            self.copies[i].start()

    def arrived(self, *which):
        for i in which:
            self.copies[i].wait_recv()

    def begin(self):
        self.start(1, 3, 0, 2, 4)

    def relay_first(self):
        self.arrived(1)
        self.start(5, 7)
        self.arrived(3)
        self.start(6, 10)

    def relay_second(self):
        self.arrived(2)
        self.start(8)
        self.arrived(4)
        self.start(9)

    def relay(self):
        self.relay_first()
        self.relay_second()

    def relay_last(self):
        self.arrived(5)
        self.start(11)
        self.arrived(6)
        self.start(12)

    def finish(self):
        for copy in self.copies:
            copy.wait_send()


def layer_kernel(
    tok_hbm, lru_w_hbm, gate_w_hbm, query_w_hbm, key_w_hbm, value_w_hbm,
    conv_ref, recur_hbm, input_hbm, rate_ref, extra_hbm, f_ref, out_lru_ref, out_fox_ref,
    o_ref,
    tok_ref, recur_ref, input_ref, extra_ref, weights, tokg, acc_kv, acc_rest, scores_a, scores_b, squares,
    kv, qb, bias, m_ref, l_ref, acc, o_send, st_send, o_relay, o_recv, st_recv,
    lru_own, halo, gate_own, decays, drives, row_tiles, col_tiles,
    lru_out, lru_g, fox_out, fox_g, w_out, acc_out, out_rows,
    send_sems, recv_sems, load_sems,
):
    sp, tp = lax.axis_index("sp"), lax.axis_index("tp")
    z, x = lax.div(sp, XS), lax.rem(sp, XS)
    y, c = lax.div(tp, 2), lax.rem(tp, 2)
    above = lax.rem(z + 1, ZS) * XS + x
    below = lax.rem(z + ZS - 1, ZS) * XS + x
    partner = y * 2 + 1 - c

    def along_y(r, core):
        return lax.rem(y + r, YS) * 2 + core

    def along_x(r):
        return z * XS + lax.rem(x + r, XS)

    def along_z(r):
        return lax.rem(z + r, ZS) * XS + x

    following, preceding = lax.rem(sp + 1, SP), lax.rem(sp + SP - 1, SP)
    used = [0]

    def copy(src, dst, **where):
        i = used[0]
        used[0] += 1
        return pltpu.make_async_remote_copy(
            src_ref=src, dst_ref=dst, send_sem=send_sems.at[i], recv_sem=recv_sems.at[i],
            device_id=where, device_id_type=MESH,
        )

    tok_load = pltpu.make_async_copy(tok_hbm, tok_ref, load_sems.at[5])
    tok_load.start()
    loads = [
        pltpu.make_async_copy(w, weights.at[i], load_sems.at[i])
        for i, w in enumerate((key_w_hbm, value_w_hbm, lru_w_hbm, query_w_hbm, gate_w_hbm))
    ]
    own_blocks = pl.ds(2 * tp, 2)
    own_columns = pl.ds(pl.multiple_of(tp * OUT, OUT), OUT)
    later_loads = [
        pltpu.make_async_copy(extra_hbm, extra_ref, load_sems.at[6]),
        pltpu.make_async_copy(recur_hbm.at[own_blocks], recur_ref, load_sems.at[7]),
        pltpu.make_async_copy(input_hbm.at[own_blocks], input_ref, load_sems.at[8]),
        pltpu.make_async_copy(out_lru_ref.at[:, own_columns], w_out.at[0, tp], load_sems.at[9]),
        pltpu.make_async_copy(out_fox_ref.at[:, own_columns], w_out.at[1, tp], load_sems.at[10]),
    ]
    for load in loads + later_loads:
        load.start()

    barrier = pltpu.get_barrier_semaphore()
    for r in range(1, TP):
        pl.semaphore_signal(
            barrier, inc=1, device_id={"tp": lax.rem(tp + r, TP)}, device_id_type=MESH
        )
    others = [along_x(r) for r in range(1, XS)] + [along_z(r) for r in range(1, ZS)]
    for other in others + [following, preceding]:
        pl.semaphore_signal(barrier, inc=1, device_id={"sp": other}, device_id_type=MESH)
    pl.semaphore_wait(barrier, TP - 1 + XS - 1 + ZS - 1 + 2)

    tokens = [
        Gather(copy, tok_ref, tokg, along_y(1, c), along_y(3, c), partner, h * HALF, HALF) for h in (0, 1)
    ]
    tok_load.wait()
    tokens[0].begin()
    forget = f_ref[...]
    high = forget.astype(jnp.bfloat16).astype(jnp.float32)
    middle = (forget - high).astype(jnp.bfloat16).astype(jnp.float32)
    low = forget - high - middle
    for h in (0, 1):
        lines = [part[2 * h : 2 * h + 2] for part in (high, middle, low)]
        kv[h, HALF:HROWS, :] = jnp.concatenate(
            lines + [jnp.zeros((10, 128), jnp.float32)], axis=0
        ).astype(jnp.bfloat16)

    def features(r, core):
        return pl.ds(pl.multiple_of(along_y(r, core) * FEAT, FEAT), FEAT)

    def pair(slot, h):
        rows = pl.ds(h * HALF, HALF)
        block = tok_ref if slot == 0 else tokg.at[slot]
        other = tokg.at[0] if slot == 0 else tokg.at[slot + 3]
        return block[rows, :], other[rows, :]

    distance = {0: 0, 1: 3, 2: 1, 3: 2}

    def project(slot, h, group, target):
        rows = [features(distance[slot], c), features(distance[slot], 1 - c)]
        right = jnp.concatenate(
            [jnp.concatenate([weights[i, part, :] for part in rows], axis=0) for i in group], axis=1
        )
        product = dot(jnp.concatenate(pair(slot, h), axis=1), right)
        half = pl.ds(h * HALF, HALF)
        target[half, :] = product if slot == 0 else target[half, :] + product

    def count_squares(slot, h):
        half = pl.ds(h * HALF, HALF)
        total = jnp.zeros((HALF, 128), jnp.float32) if slot == 0 else squares[half, :]
        for piece in pair(slot, h):
            for g in range(FEAT // 128):
                value = piece[:, g * 128 : (g + 1) * 128].astype(jnp.float32)
                total = total + value * value
        squares[half, :] = total

    def take(slot, h):
        project(slot, h, (0, 1, 2), acc_kv)
        project(slot, h, (3, 4), acc_rest)
        count_squares(slot, h)

    plus = [(0, 2), (1, 3), (2, 4), (3, 5), (4, 6), (5, 7), (6, 14)]
    minus = [(0, 8), (1, 9), (8, 10), (9, 11), (10, 12), (11, 13), (13, 15)]
    plus = [copy(kv.at[a], kv.at[b], sp=above) for a, b in plus]
    minus = [copy(kv.at[a], kv.at[b], sp=below) for a, b in minus]
    tail = copy(lru_own.at[pl.ds(BLK - 16, 16)], halo, sp=following)
    query_rows = [pl.ds(pl.multiple_of(x * BLK + h * HALF, HALF), HALF) for h in (0, 1)]
    query_copies = [
        {r: copy(qb.at[rows], qb.at[rows], sp=along_x(r)) for r in (1, 2, 3)} for rows in query_rows
    ]

    def conclude(h):
        half = pl.ds(h * HALF, HALF)
        count_squares(3, h)
        row_scale = lax.rsqrt(
            jnp.sum(squares[half, :], axis=1, keepdims=True) * (1.0 / D) + epsilon_norm
        )
        project(3, h, (0, 1, 2), acc_kv)
        ready = (acc_kv[half, :] * row_scale).astype(jnp.bfloat16)
        lru_own[half, :] = ready[:, 256:]
        if h == 1:
            tail.start()
        kv[h, :HALF, :] = ready[:, :128]
        kv[h, HROWS:, :] = ready[:, 128:256]
        plus[h].start()
        minus[h].start()
        project(3, h, (3, 4), acc_rest)
        rest = (acc_rest[half, :] * row_scale).astype(jnp.bfloat16)
        qb[query_rows[h], :] = rest[:, :128]
        gate_own[half, :] = rest[:, 128:]
        for r in (1, 3, 2):
            query_copies[h][r].start()

    for load in loads:
        load.wait()
    early, late = tokens
    early.arrived(0)
    take(0, 0)
    early.relay_first()
    late.begin()
    early.relay_second()
    early.arrived(7, 8)
    take(1, 0)
    early.arrived(9, 10)
    take(2, 0)
    early.relay_last()
    late.arrived(0)
    take(0, 1)
    late.relay_first()
    early.arrived(11, 12)
    conclude(0)
    late.relay_second()
    late.arrived(7, 8)
    take(1, 1)
    late.arrived(9, 10)
    take(2, 1)
    late.relay_last()
    late.arrived(11, 12)
    conclude(1)

    weight_copies = []
    for r in range(1, TP):
        to = lax.rem(tp + r, TP)
        columns = pl.ds(pl.multiple_of(to * OUT, OUT), OUT)
        for k, ref in enumerate((out_lru_ref, out_fox_ref)):
            weight_copies.append(copy(ref.at[:, columns], w_out.at[k, tp], tp=to))
    for each in weight_copies:
        each.start()
    own_rows = pl.ds(pl.multiple_of(x * BLK, BLK), BLK)
    m_ref[...] = jnp.full_like(m_ref, NEG)
    l_ref[...] = jnp.zeros_like(l_ref)
    acc[...] = jnp.zeros_like(acc)

    def set_bias(slot):
        parts = kv[slot, HALF:HROWS, :].astype(jnp.float32)
        whole = parts[0:2] + parts[2:4] + parts[4:6]
        for g in range(2):
            bias[slot : slot + 1, g * 128 : (g + 1) * 128] = whole[g : g + 1] * -LOG2E

    scale = HEAD_DIM ** (-0.5) * LOG2E

    def joint(parts, axis):
        return parts[0] if len(parts) == 1 else jnp.concatenate(parts, axis=axis)

    def score(buffer, i, slots):
        rows = pl.ds(pl.multiple_of(i * BLK, BLK), BLK)
        buffer[:, : HALF * len(slots)] = lax.dot_general(
            qb[rows, :],
            joint([kv[slot, :HALF, :] for slot in slots], 0),
            (((1,), (1,)), ((), ())),
            preferred_element_type=jnp.float32,
        )

    def absorb(buffer, i, slots, masked=False):
        rows = pl.ds(pl.multiple_of(i * BLK, BLK), BLK)
        width = HALF * len(slots)
        offsets = joint([bias[slot : slot + 1, :] for slot in slots], 1)
        scores = buffer[:, :width] * scale + offsets
        if masked:
            earlier = lax.broadcasted_iota(jnp.int32, scores.shape, 0) >= lax.broadcasted_iota(
                jnp.int32, scores.shape, 1
            )
            scores = jnp.where(earlier, scores, NEG)
        old = m_ref[rows, :]
        new = jnp.maximum(old, jnp.max(scores, axis=1, keepdims=True))
        rescale = jnp.exp2(old - new)
        probs = jnp.exp2(scores - jnp.concatenate([new] * (width // 128), axis=1))
        total = l_ref[rows, :] * rescale
        for g in range(width // 128):
            total = total + probs[:, g * 128 : (g + 1) * 128]
        l_ref[rows, :] = total
        m_ref[rows, :] = new
        acc[rows, :] = acc[rows, :] * rescale + dot(
            probs.astype(jnp.bfloat16), joint([kv[slot, HROWS:, :] for slot in slots], 0)
        )

    def attend(i, slots, masked=False):
        score(scores_a, i, slots)
        absorb(scores_a, i, slots, masked)

    def visit_rest(slots, first):
        def body(i, carry):
            attend(i, slots)
            return carry

        lax.fori_loop(first, XS, body, 0)

    def visit(*slots):
        for slot in slots:
            set_bias(slot)
        score(scores_a, 0, slots)

        def body(k, carry):
            score(scores_b, 2 * k + 1, slots)
            absorb(scores_a, 2 * k, slots)
            score(scores_a, jnp.minimum(2 * k + 2, XS - 1), slots)
            absorb(scores_b, 2 * k + 1, slots)
            return carry

        lax.fori_loop(0, XS // 2, body, 0)

    def receive(i):
        plus[i].wait_recv()
        if i < 5:
            plus[i + 2].start()
        minus[i].wait_recv()
        if i < 4:
            minus[i + 2].start()
        elif i == 5:
            minus[6].start()

    def take_keys(i):
        d = i // 2 + 1
        if d == 4:

            @pl.when(z >= 4)
            def _():
                visit(14, 15)

            return

        @pl.when(z + d >= ZS)
        def _():
            visit(i + 2, i + 8)

        @pl.when((z >= d) & (z + d < ZS))
        def _():
            visit(i + 2)

    set_bias(0)
    set_bias(1)
    attend(x, (0, 1), masked=True)
    receive(0)

    tail.wait_recv()
    for load in later_loads:
        load.wait()
    lru_input = lru_own[...].astype(jnp.float32)
    before = halo[8:16, :].astype(jnp.float32) * jnp.where(sp > 0, 1.0, 0.0)
    joined = jnp.concatenate([before, lru_input], axis=0)
    channels = pl.ds(pl.multiple_of(tp * 128, 128), 128)
    taps = conv_ref[:, channels].astype(jnp.float32)
    conv = jnp.zeros((BLK, 128), jnp.float32)
    for j in range(4):
        shifted = joined if j == 3 else pltpu.roll(joined, 3 - j, 0)
        conv = conv + taps[j : j + 1, :] * shifted[8:, :]
    conv = conv.astype(jnp.bfloat16)
    column = lax.broadcasted_iota(jnp.int32, (64, 128), 1)
    row = lax.broadcasted_iota(jnp.int32, (64, 128), 0)
    left = jnp.where(column == row, 1.0, 0.0).astype(jnp.bfloat16)
    right = jnp.where(column == row + 64, 1.0, 0.0).astype(jnp.bfloat16)

    def block_diagonal(ref):
        return jnp.concatenate([dot(ref[0], left), dot(ref[1], right)], axis=0)

    gates_w = jnp.concatenate([block_diagonal(recur_ref), block_diagonal(input_ref)], axis=1)
    gates = dot(conv, gates_w.astype(jnp.bfloat16))
    gates = 1.0 / (1.0 + jnp.exp(-gates))
    rate = log1p_unit(jnp.exp(-rate_ref[pl.ds(tp, 1), :]))
    log_decay = (-decay_sharpness * rate) * gates[:, :128] + extra_ref[...]
    drive = jnp.sqrt(minus_expm1(2.0 * log_decay)) * gates[:, 128:] * conv.astype(jnp.float32)
    decay = jnp.exp(log_decay)
    place = lax.broadcasted_iota(jnp.int32, (BLK, 128), 0)
    step = 1
    while step < BLK:
        if step < 8:
            inside = place >= step
            decay_back = jnp.where(inside, pltpu.roll(decay, step, 0), 1.0)
            drive_back = jnp.where(inside, pltpu.roll(drive, step, 0), 0.0)
        else:
            decay_back = jnp.concatenate([jnp.ones((step, 128), jnp.float32), decay[:-step]], axis=0)
            drive_back = jnp.concatenate([jnp.zeros((step, 128), jnp.float32), drive[:-step]], axis=0)
        drive = decay * drive_back + drive
        decay = decay * decay_back
        step *= 2
    decays[...] = decay
    drives[...] = drive

    def tile_of(a, b):
        return jnp.concatenate([a, b, jnp.zeros((6, 128), jnp.float32)], axis=0)

    row_tiles[0] = tile_of(decays[BLK - 1 :, :], drives[BLK - 1 :, :])
    row_copies = {r: copy(row_tiles.at[0], row_tiles.at[r], sp=along_x(r)) for r in (1, 2, 3)}
    for r in (1, 3, 2):
        row_copies[r].start()

    receive(1)
    for queries in query_copies:
        for r in (1, 3, 2):
            queries[r].wait_recv()
    visit_rest((0, 1), x + 1)

    column_copies = {r: copy(col_tiles.at[0], col_tiles.at[r], sp=along_z(r)) for r in range(1, ZS)}
    branch = Gather(copy, lru_out, lru_g, along_y(1, c), along_y(3, c), partner)
    one, zero = jnp.ones((1, 128), jnp.float32), jnp.zeros((1, 128), jnp.float32)

    def total_of_row():
        for r in (1, 3, 2):
            row_copies[r].wait_recv()
        whole_decay, whole_state, state = one, zero, zero
        for k in range(XS):
            block = row_tiles[lax.rem(x + XS - k, XS)]
            a, b = block[0:1], block[1:2]
            state = jnp.where(k < x, a * state + b, state)
            whole_state = a * whole_state + b
            whole_decay = whole_decay * a
        col_tiles[0] = tile_of(whole_decay, whole_state)
        for r in range(1, ZS):
            column_copies[r].start()

    def recurrence_out():
        for r in range(1, ZS):
            column_copies[r].wait_recv()
        state = zero
        for k in range(ZS):
            block = col_tiles[lax.rem(z + ZS - k, ZS)]
            state = jnp.where(k < z, block[0:1] * state + block[1:2], state)
        for k in range(XS):
            block = row_tiles[lax.rem(x + XS - k, XS)]
            state = jnp.where(k < x, block[0:1] * state + block[1:2], state)
        gate = gate_own[...].astype(jnp.float32)
        inner = 0.7978845608028654 * (gate + 0.044715 * gate * gate * gate)
        gelu = 0.5 * gate * (1.0 + jnp.tanh(inner))
        lru_out[...] = ((drives[...] + decays[...] * state) * gelu).astype(jnp.bfloat16)
        branch.begin()

    beside = {0: total_of_row, 2: recurrence_out, 4: branch.relay}
    for i in range(7):
        take_keys(i)
        if i in beside:
            beside[i]()
        if i < 4:
            receive(i + 2)
        elif i == 5:
            receive(6)

    right, left = along_x(1), along_x(3)
    out_copies = []
    for h in (0, 1):
        rows = pl.ds(h * HALF, HALF)
        quarters = [pl.ds(h * HALF + k * 128, 128) for k in (0, 1)]
        out_copies.append(
            {
                "relay": [
                    copy(o_send.at[2, part], o_relay.at[k, part], sp=to)
                    for k, (part, to) in enumerate(zip(quarters, (right, left)))
                ],
                "near": [copy(o_send.at[r, rows], o_recv.at[r, rows], sp=along_x(r)) for r in (1, 3)],
                "far": [
                    copy(o_relay.at[k, part], o_recv.at[2, part], sp=to)
                    for k, (part, to) in enumerate(zip(quarters, (right, left)))
                ],
            }
        )
    stat_copies = [copy(st_send.at[r], st_recv.at[r], sp=along_x(r)) for r in (1, 2, 3)]

    def stats(rows):
        total = jnp.broadcast_to(jnp.sum(l_ref[rows, :], axis=1, keepdims=True), (BLK, 128))
        return packed_rows(m_ref[rows, :]), packed_rows(total)

    def send_out(h, kind):
        for each in out_copies[h][kind]:
            each.start()

    def got_out(h, kind):
        for each in out_copies[h][kind]:
            each.wait_recv()

    def rows_of(r):
        return pl.ds(pl.multiple_of(lax.rem(x + r, XS) * BLK, BLK), BLK)

    o_send[2] = acc[rows_of(2), :].astype(jnp.bfloat16)
    send_out(0, "relay")
    for r in (1, 3):
        o_send[r] = acc[rows_of(r), :].astype(jnp.bfloat16)
    send_out(0, "near")
    send_out(1, "relay")
    for r in (1, 2, 3):
        st_send[r] = jnp.concatenate(stats(rows_of(r)), axis=0)
    for each in stat_copies:
        each.start()
    tops, sums = [None] * 4, [None] * 4
    tops[0], sums[0] = stats(own_rows)
    branch.relay_last()

    got_out(0, "relay")
    send_out(0, "far")
    send_out(1, "near")

    sources = [(0, c), (0, 1 - c), (3, c), (3, 1 - c), (1, c), (1, 1 - c), (2, c), (2, 1 - c)]

    def branch_product(k, own, slots, which, rows):
        lookup = [None, 0, 1, 4, 2, 5, 3, 6]
        blocks = [own[rows, :] if lookup[i] is None else slots[lookup[i], rows, :] for i in which]
        rights = [w_out[k, along_y(*sources[i])] for i in which]
        return dot(jnp.concatenate(blocks, axis=1), jnp.concatenate(rights, axis=0))

    for each in weight_copies:
        each.wait_recv()
    branch.arrived(0, 7, 8, 9, 10, 11, 12)
    got_out(1, "relay")
    send_out(1, "far")
    acc_out[...] = branch_product(0, lru_out, lru_g, range(8), pl.ds(0, BLK))

    for each in stat_copies:
        each.wait_recv()
    for r in (1, 2, 3):
        both = st_recv[r]
        tops[r], sums[r] = both[0:4], both[4:8]
    top = jnp.maximum(jnp.maximum(tops[0], tops[1]), jnp.maximum(tops[2], tops[3]))
    shares = [jnp.exp2(t - top) for t in tops]
    whole = shares[0] * sums[0] + shares[1] * sums[1] + shares[2] * sums[2] + shares[3] * sums[3]
    shares = [s / whole for s in shares]
    heads = [
        Gather(copy, fox_out, fox_g, along_y(1, c), along_y(3, c), partner, h * HALF, HALF) for h in (0, 1)
    ]

    def merge(h):
        got_out(h, "near")
        got_out(h, "far")
        for g in (2 * h, 2 * h + 1):
            part = pl.ds(g * 128, 128)
            mine = pl.ds(pl.multiple_of(x * BLK + g * 128, 128), 128)
            total = unpacked_row(shares[0][g : g + 1]) * acc[mine, :]
            for r in (1, 2, 3):
                total = total + unpacked_row(shares[r][g : g + 1]) * o_recv[r, part, :].astype(jnp.float32)
            fox_out[part, :] = total.astype(jnp.bfloat16)
        heads[h].begin()

    def head_product(h, which):
        rows = pl.ds(h * HALF, HALF)
        return branch_product(1, fox_out, fox_g, which, rows)

    halves = [pl.ds(h * HALF, HALF) for h in (0, 1)]
    out_loads = [
        pltpu.make_async_copy(out_rows.at[half], o_ref.at[half], load_sems.at[11 + h])
        for h, half in enumerate(halves)
    ]

    def write(h):
        heads[h].arrived(11, 12)
        out_rows[halves[h], :] = (acc_out[halves[h], :] + head_product(h, (6, 7))).astype(out_rows.dtype)
        out_loads[h].start()

    merge(0)
    merge(1)
    heads[0].relay()
    heads[0].arrived(0)
    acc_out[halves[0], :] += head_product(0, (0, 1))
    heads[1].relay_first()
    heads[0].relay_last()
    heads[1].relay_second()
    heads[1].arrived(0)
    acc_out[halves[1], :] += head_product(1, (0, 1))
    heads[0].arrived(7, 8, 9, 10)
    acc_out[halves[0], :] += head_product(0, (2, 3, 4, 5))
    write(0)
    heads[1].relay_last()
    heads[1].arrived(7, 8, 9, 10)
    acc_out[halves[1], :] += head_product(1, (2, 3, 4, 5))
    write(1)

    for each in plus + minus + [tail] + weight_copies + stat_copies:
        each.wait_send()
    for group in query_copies + [row_copies, column_copies]:
        for each in group.values():
            each.wait_send()
    for group in out_copies:
        for kind in group.values():
            for each in kind:
                each.wait_send()
    for group in tokens + [branch] + heads:
        group.finish()
    for each in out_loads:
        each.wait()


def layer(
    tokens, lru_in, lru_gate_in, query_w, key_w, value_w, conv_weight, recur_gate_w, input_gate_w,
    rate_param, decay_extra, forget_cum, out_lru, out_fox,
):
    vmem = pl.BlockSpec(memory_space=pltpu.VMEM)
    hbm = pl.BlockSpec(memory_space=pl.ANY)
    bf16, f32 = jnp.bfloat16, jnp.float32
    return pl.pallas_call(
        layer_kernel,
        out_shape=jax.ShapeDtypeStruct((BLK, OUT), bf16),
        in_specs=[hbm] * 6 + [vmem, hbm, hbm, vmem, hbm, vmem, hbm, hbm],
        out_specs=hbm,
        scratch_shapes=[
            pltpu.VMEM((BLK, FEAT), bf16),
            pltpu.VMEM((2, 64, 64), bf16),
            pltpu.VMEM((2, 64, 64), bf16),
            pltpu.VMEM((BLK, 128), f32),
            pltpu.VMEM((5, D, 128), bf16),
            pltpu.VMEM((7, BLK, FEAT), bf16),
            pltpu.VMEM((BLK, 384), f32),
            pltpu.VMEM((BLK, 256), f32),
            pltpu.VMEM((BLK, BLK), f32),
            pltpu.VMEM((BLK, BLK), f32),
            pltpu.VMEM((BLK, 128), f32),
            pltpu.VMEM((2 * ZS, PIECE, 128), bf16),
            pltpu.VMEM((XS * BLK, 128), bf16),
            pltpu.VMEM((2 * ZS, HALF), f32),
            pltpu.VMEM((XS * BLK, 128), f32),
            pltpu.VMEM((XS * BLK, 128), f32),
            pltpu.VMEM((XS * BLK, 128), f32),
            pltpu.VMEM((XS, BLK, 128), bf16),
            pltpu.VMEM((XS, 8, 128), f32),
            pltpu.VMEM((2, BLK, 128), bf16),
            pltpu.VMEM((XS, BLK, 128), bf16),
            pltpu.VMEM((XS, 8, 128), f32),
            pltpu.VMEM((BLK, 128), bf16),
            pltpu.VMEM((16, 128), bf16),
            pltpu.VMEM((BLK, 128), bf16),
            pltpu.VMEM((BLK, 128), f32),
            pltpu.VMEM((BLK, 128), f32),
            pltpu.VMEM((XS, 8, 128), f32),
            pltpu.VMEM((ZS, 8, 128), f32),
            pltpu.VMEM((BLK, 128), bf16),
            pltpu.VMEM((7, BLK, 128), bf16),
            pltpu.VMEM((BLK, 128), bf16),
            pltpu.VMEM((7, BLK, 128), bf16),
            pltpu.VMEM((2, TP, 128, OUT), bf16),
            pltpu.VMEM((BLK, OUT), f32),
            pltpu.VMEM((BLK, OUT), bf16),
            pltpu.SemaphoreType.DMA((COPIES,)),
            pltpu.SemaphoreType.DMA((COPIES,)),
            pltpu.SemaphoreType.DMA((13,)),
        ],
        compiler_params=pltpu.CompilerParams(collective_id=1, has_side_effects=True),
        cost_estimate=pl.CostEstimate(flops=5_000_000_000, bytes_accessed=8_000_000, transcendentals=9_000_000),
    )(
        tokens, lru_in, lru_gate_in, query_w, key_w, value_w, conv_weight, recur_gate_w, input_gate_w,
        rate_param.reshape(TP, 128), decay_extra, forget_cum.reshape(4, 128), out_lru, out_fox,
    )


def solution(mesh):
    placed = (
        P("sp", "tp"),
        P(None, "tp"),
        P(None, "tp"),
        P(None, "tp"),
        P(None, "tp"),
        P(None, "tp"),
        P(),
        P(),
        P(),
        P(),
        P("sp", "tp"),
        P("sp", "tp"),
        P("tp", None),
        P("tp", None),
    )
    return jax.shard_map(
        layer, mesh=mesh, in_specs=placed, out_specs=P("sp", "tp"), check_vma=False
    )
```

time: 72.4 us -> 69 us (0.953)
  the two profiles are of different devices: /device:TPU:11 before, /device:TPU:1 now
where the time goes in v3:
time: 69 us; the launch traced here: 68.9 us
  Pallas kernels  67.2 us (97%)
  local copies, waits for them, and re-layouts  1.67 us (2%)
    pallas_call x1, Pallas kernels, layer(): pl.pallas_call(layer_kernel, out_shape=jax.ShapeDtypeStruct((BLK, OUT), b...  67.2 us
    unnamed x1, local copies, waits for them, and re-layouts  1.67 us

profile of v3, /device:TPU:1, one launch (start us, length us, event | category | flops | bytes accessed | tf_op | source)
XLA Modules:
  0.0 68.9 jit_solution(15725481795627215373)
XLA Ops:
  0.0 67.2 %shard_map.136 = bf16[512,256]{1,0:T(8,128)(2,1)} custom-call(bf16[512,256]{1,0:T(8,128)(2,1)} %tok_hbm.1, bf16[2048,128]{1,0:T(8,128)(2,1)} %lru_w_hbm.1, bf16[2048,128]{1,0:T(8,128)(2,1)} %gate_w_hbm.1, bf16[2048,128]{1,0:T(8,128)(2,1)} %query_w_hbm.1, bf16[2048,128]{1,0:T(8,128)(2,1)} %key_w_hbm.1, bf16[2048,128]{1,0:T(8,128)(2,1)} %value_w_hbm.1, ...), custom_call_target="tpu_custom_call" | custom-call | flops 5000000000 | bytes 8000000 | tf_op jit(solution)/shard_map/pallas_call | solution.py:670
  67.2 1.7 %copy.16 = bf16[512,256]{1,0:T(8,128)(2,1)} copy(bf16[512,256]{1,0:T(8,128)(2,1)} %shard_map.136) | data formatting | bytes 524288

commit v4 on v3

--- a/solution.py
+++ b/solution.py
@@ -138,7 +138,7 @@
     kv, qb, bias, m_ref, l_ref, acc, o_send, st_send, o_relay, o_recv, st_recv,
     lru_own, halo, gate_own, decays, drives, row_tiles, col_tiles,
     lru_out, lru_g, fox_out, fox_g, w_out, acc_out, out_rows,
-    send_sems, recv_sems, load_sems,
+    send_sems, recv_sems, load_sems, alive,
 ):
     sp, tp = lax.axis_index("sp"), lax.axis_index("tp")
     z, x = lax.div(sp, XS), lax.rem(sp, XS)
@@ -186,14 +186,37 @@
         load.start()
 
     barrier = pltpu.get_barrier_semaphore()
+
+    def tell(semaphore, **where):
+        pl.semaphore_signal(semaphore, inc=1, device_id=where, device_id_type=MESH)
+
     for r in range(1, TP):
-        pl.semaphore_signal(
-            barrier, inc=1, device_id={"tp": lax.rem(tp + r, TP)}, device_id_type=MESH
-        )
-    others = [along_x(r) for r in range(1, XS)] + [along_z(r) for r in range(1, ZS)]
-    for other in others + [following, preceding]:
-        pl.semaphore_signal(barrier, inc=1, device_id={"sp": other}, device_id_type=MESH)
-    pl.semaphore_wait(barrier, TP - 1 + XS - 1 + ZS - 1 + 2)
+        tell(barrier, tp=lax.rem(tp + r, TP))
+    for r in range(1, XS):
+        tell(barrier, sp=along_x(r))
+    for r in range(1, ZS):
+
+        @pl.when(z + r < ZS)
+        def _():
+            tell(barrier, sp=along_z(r))
+
+    last_of_row = (x == XS - 1) & (z < ZS - 1)
+    first_of_row = (x == 0) & (z > 0)
+
+    @pl.when(last_of_row)
+    def _():
+        tell(barrier, sp=following)
+
+    pl.semaphore_wait(barrier, TP - 1 + XS - 1 + z + first_of_row.astype(jnp.int32))
+    for r in range(1, ZS):
+
+        @pl.when(z >= r)
+        def _():
+            tell(alive, sp=along_z(ZS - r))
+
+    @pl.when(first_of_row)
+    def _():
+        tell(alive, sp=preceding)
 
     tokens = [
         Gather(copy, tok_ref, tokg, along_y(1, c), along_y(3, c), partner, h * HALF, HALF) for h in (0, 1)
@@ -244,10 +267,24 @@
         project(slot, h, (3, 4), acc_rest)
         count_squares(slot, h)
 
-    plus = [(0, 2), (1, 3), (2, 4), (3, 5), (4, 6), (5, 7), (6, 14)]
-    minus = [(0, 8), (1, 9), (8, 10), (9, 11), (10, 12), (11, 13), (13, 15)]
+    plus = [(0, 2), (1, 3), (2, 4), (3, 5), (4, 6), (5, 7)]
+    minus = [(0, 8), (1, 9), (8, 10), (9, 11), (10, 12), (11, 13), (12, 14), (13, 15)]
     plus = [copy(kv.at[a], kv.at[b], sp=above) for a, b in plus]
     minus = [copy(kv.at[a], kv.at[b], sp=below) for a, b in minus]
+
+    def wrapped(d):
+        return lax.rem(z + d, ZS) < 4
+
+    def send_plus(i):
+        @pl.when((z < ZS - 1) & (z >= i // 2))
+        def _():
+            plus[i].start()
+
+    def send_minus(i):
+        @pl.when(wrapped(i // 2))
+        def _():
+            minus[i].start()
+
     tail = copy(lru_own.at[pl.ds(BLK - 16, 16)], halo, sp=following)
     query_rows = [pl.ds(pl.multiple_of(x * BLK + h * HALF, HALF), HALF) for h in (0, 1)]
     query_copies = [
@@ -263,12 +300,23 @@
         project(3, h, (0, 1, 2), acc_kv)
         ready = (acc_kv[half, :] * row_scale).astype(jnp.bfloat16)
         lru_own[half, :] = ready[:, 256:]
-        if h == 1:
-            tail.start()
+        if h == 0:
+            later = (ZS - 1 - z) + last_of_row.astype(jnp.int32)
+
+            @pl.when(later > 0)
+            def _():
+                pl.semaphore_wait(alive, later)
+
+        else:
+
+            @pl.when(sp < SP - 1)
+            def _():
+                tail.start()
+
         kv[h, :HALF, :] = ready[:, :128]
         kv[h, HROWS:, :] = ready[:, 128:256]
-        plus[h].start()
-        minus[h].start()
+        send_plus(h)
+        send_minus(h)
         project(3, h, (3, 4), acc_rest)
         rest = (acc_rest[half, :] * row_scale).astype(jnp.bfloat16)
         qb[query_rows[h], :] = rest[:, :128]
@@ -385,14 +433,21 @@
         lax.fori_loop(0, XS // 2, body, 0)
 
     def receive(i):
-        plus[i].wait_recv()
-        if i < 5:
-            plus[i + 2].start()
-        minus[i].wait_recv()
-        if i < 4:
-            minus[i + 2].start()
-        elif i == 5:
-            minus[6].start()
+        d = i // 2 + 1
+        if d < 4:
+
+            @pl.when(z >= d)
+            def _():
+                plus[i].wait_recv()
+
+            if d < 3:
+                send_plus(i + 2)
+
+        @pl.when(wrapped(d))
+        def _():
+            minus[i].wait_recv()
+            if d < 4:
+                minus[i + 2].start()
 
     def take_keys(i):
         d = i // 2 + 1
@@ -417,11 +472,18 @@
     attend(x, (0, 1), masked=True)
     receive(0)
 
-    tail.wait_recv()
+    @pl.when(sp > 0)
+    def _():
+        tail.wait_recv()
+
+    @pl.when(sp == 0)
+    def _():
+        halo[...] = jnp.zeros_like(halo)
+
     for load in later_loads:
         load.wait()
     lru_input = lru_own[...].astype(jnp.float32)
-    before = halo[8:16, :].astype(jnp.float32) * jnp.where(sp > 0, 1.0, 0.0)
+    before = halo[8:16, :].astype(jnp.float32)
     joined = jnp.concatenate([before, lru_input], axis=0)
     channels = pl.ds(pl.multiple_of(tp * 128, 128), 128)
     taps = conv_ref[:, channels].astype(jnp.float32)
@@ -491,15 +553,23 @@
             whole_decay = whole_decay * a
         col_tiles[0] = tile_of(whole_decay, whole_state)
         for r in range(1, ZS):
-            column_copies[r].start()
+
+            @pl.when(z + r < ZS)
+            def _():
+                column_copies[r].start()
 
     def recurrence_out():
         for r in range(1, ZS):
-            column_copies[r].wait_recv()
-        state = zero
-        for k in range(ZS):
-            block = col_tiles[lax.rem(z + ZS - k, ZS)]
-            state = jnp.where(k < z, block[0:1] * state + block[1:2], state)
+
+            @pl.when(z >= r)
+            def _():
+                column_copies[r].wait_recv()
+
+        def row_above(k, state):
+            block = col_tiles[z - k]
+            return block[0:1] * state + block[1:2]
+
+        state = lax.fori_loop(0, z, row_above, zero)
         for k in range(XS):
             block = row_tiles[lax.rem(x + XS - k, XS)]
             state = jnp.where(k < x, block[0:1] * state + block[1:2], state)
@@ -516,8 +586,10 @@
             beside[i]()
         if i < 4:
             receive(i + 2)
+        elif i == 4:
+            receive(6)
         elif i == 5:
-            receive(6)
+            receive(7)
 
     right, left = along_x(1), along_x(3)
     out_copies = []
@@ -645,9 +717,31 @@
     acc_out[halves[1], :] += head_product(1, (2, 3, 4, 5))
     write(1)
 
-    for each in plus + minus + [tail] + weight_copies + stat_copies:
+    for i, each in enumerate(plus):
+
+        @pl.when((z < ZS - 1) & (z >= i // 2))
+        def _():
+            each.wait_send()
+
+    for i, each in enumerate(minus):
+
+        @pl.when(wrapped(i // 2))
+        def _():
+            each.wait_send()
+
+    @pl.when(sp < SP - 1)
+    def _():
+        tail.wait_send()
+
+    for r in range(1, ZS):
+
+        @pl.when(z + r < ZS)
+        def _():
+            column_copies[r].wait_send()
+
+    for each in weight_copies + stat_copies:
         each.wait_send()
-    for group in query_copies + [row_copies, column_copies]:
+    for group in query_copies + [row_copies]:
         for each in group.values():
             each.wait_send()
     for group in out_copies:
@@ -712,6 +806,7 @@
             pltpu.SemaphoreType.DMA((COPIES,)),
             pltpu.SemaphoreType.DMA((COPIES,)),
             pltpu.SemaphoreType.DMA((13,)),
+            pltpu.SemaphoreType.REGULAR,
         ],
         compiler_params=pltpu.CompilerParams(collective_id=1, has_side_effects=True),
         cost_estimate=pl.CostEstimate(flops=5_000_000_000, bytes_accessed=8_000_000, transcendentals=9_000_000),

time: 69 us -> 67 us (0.971)
  the two profiles are of different devices: /device:TPU:1 before, /device:TPU:193 now
where the time goes in v4:
time: 67 us; the launch traced here: 66.8 us
  Pallas kernels  65.1 us (97%)
  local copies, waits for them, and re-layouts  1.67 us (2%)
    pallas_call x1, Pallas kernels, layer(): pl.pallas_call(layer_kernel, out_shape=jax.ShapeDtypeStruct((BLK, OUT), b...  65.1 us
    unnamed x1, local copies, waits for them, and re-layouts  1.67 us

profile of v4, /device:TPU:193, one launch (start us, length us, event | category | flops | bytes accessed | tf_op | source)
XLA Modules:
  0.0 66.8 jit_solution(13335508612410709703)
XLA Ops:
  0.0 65.1 %shard_map.136 = bf16[512,256]{1,0:T(8,128)(2,1)} custom-call(bf16[512,256]{1,0:T(8,128)(2,1)} %tok_hbm.1, bf16[2048,128]{1,0:T(8,128)(2,1)} %lru_w_hbm.1, bf16[2048,128]{1,0:T(8,128)(2,1)} %gate_w_hbm.1, bf16[2048,128]{1,0:T(8,128)(2,1)} %query_w_hbm.1, bf16[2048,128]{1,0:T(8,128)(2,1)} %key_w_hbm.1, bf16[2048,128]{1,0:T(8,128)(2,1)} %value_w_hbm.1, ...), custom_call_target="tpu_custom_call" | custom-call | flops 5000000000 | bytes 8000000 | tf_op jit(solution)/shard_map/pallas_call | solution.py:764
  65.1 1.7 %copy.16 = bf16[512,256]{1,0:T(8,128)(2,1)} copy(bf16[512,256]{1,0:T(8,128)(2,1)} %shard_map.136) | data formatting | bytes 524288

commit v5 on v4

--- a/solution.py
+++ b/solution.py
@@ -18,7 +18,7 @@
 PIECE = HROWS + HALF
 LOG2E = 1.4426950408889634
 NEG = -1e30
-COPIES = 152
+COPIES = 96
 
 decay_sharpness = 8.0
 epsilon_norm = 1e-06
@@ -67,30 +67,36 @@
     return jnp.where(x > -0.5, -near * x, 1.0 - jnp.exp(x))
 
 
+def await_bytes(ref, semaphore):
+    pltpu.make_async_copy(ref, ref, semaphore).wait()
+
+
 class Gather:
-    def __init__(self, copy, own, slots, up, down, partner, start=0, rows=BLK):
+    def __init__(self, copy, sems, own, slots, up, down, partner, start=0, rows=BLK):
         half = rows // 2
         first, second = pl.ds(start, half), pl.ds(start + half, half)
 
-        def send(a, b, part, to):
+        def send(a, b, part, to, k):
             source = own if a is None else slots.at[a]
-            return copy(source.at[part], slots.at[b, part], tp=to)
-
-        self.copies = [
-            send(None, 0, pl.ds(start, rows), partner),
-            send(None, 1, first, up),
-            send(None, 1, second, up),
-            send(None, 2, second, down),
-            send(None, 2, first, down),
-            send(1, 3, first, up),
-            send(2, 3, second, down),
-            send(1, 4, first, partner),
-            send(1, 4, second, partner),
-            send(2, 5, first, partner),
-            send(2, 5, second, partner),
-            send(3, 6, first, partner),
-            send(3, 6, second, partner),
+            return copy(source.at[part], slots.at[b, part], send=sems[10], recv=sems[k], tp=to)
+
+        plan = [
+            (None, 0, pl.ds(start, rows), partner, 0),
+            (None, 1, first, up, 1),
+            (None, 1, second, up, 2),
+            (None, 2, second, down, 3),
+            (None, 2, first, down, 4),
+            (1, 3, first, up, 5),
+            (2, 3, second, down, 6),
+            (1, 4, first, partner, 7),
+            (1, 4, second, partner, 7),
+            (2, 5, first, partner, 8),
+            (2, 5, second, partner, 8),
+            (3, 6, first, partner, 9),
+            (3, 6, second, partner, 9),
         ]
+        self.copies = [send(*each) for each in plan]
+        self.sems, self.slots, self.rows = sems, slots, pl.ds(start, rows)
 
     def start(self, *which):
         for i in which:
@@ -99,6 +105,13 @@
     def arrived(self, *which):
         for i in which:
             self.copies[i].wait_recv()
+
+    def arrived_from_partner(self, *slots):
+        for slot in slots:
+            await_bytes(self.slots.at[slot, self.rows], self.sems[slot + 3])
+
+    def finish(self):
+        await_bytes(self.slots.at[:, self.rows], self.sems[10])
 
     def begin(self):
         self.start(1, 3, 0, 2, 4)
@@ -124,10 +137,6 @@
         self.start(11)
         self.arrived(6)
         self.start(12)
-
-    def finish(self):
-        for copy in self.copies:
-            copy.wait_send()
 
 
 def layer_kernel(
@@ -138,7 +147,7 @@
     kv, qb, bias, m_ref, l_ref, acc, o_send, st_send, o_relay, o_recv, st_recv,
     lru_own, halo, gate_own, decays, drives, row_tiles, col_tiles,
     lru_out, lru_g, fox_out, fox_g, w_out, acc_out, out_rows,
-    send_sems, recv_sems, load_sems, alive,
+    copy_sems, load_sems, alive,
 ):
     sp, tp = lax.axis_index("sp"), lax.axis_index("tp")
     z, x = lax.div(sp, XS), lax.rem(sp, XS)
@@ -159,28 +168,32 @@
     following, preceding = lax.rem(sp + 1, SP), lax.rem(sp + SP - 1, SP)
     used = [0]
 
-    def copy(src, dst, **where):
-        i = used[0]
+    def semaphore():
         used[0] += 1
+        return copy_sems.at[used[0] - 1]
+
+    def copy(src, dst, send=None, recv=None, **where):
         return pltpu.make_async_remote_copy(
-            src_ref=src, dst_ref=dst, send_sem=send_sems.at[i], recv_sem=recv_sems.at[i],
+            src_ref=src, dst_ref=dst, send_sem=send or semaphore(), recv_sem=recv or semaphore(),
             device_id=where, device_id_type=MESH,
         )
 
-    tok_load = pltpu.make_async_copy(tok_hbm, tok_ref, load_sems.at[5])
+    gather_sems = [[semaphore() for k in range(11)] for group in range(3)]
+
+    tok_load = pltpu.make_async_copy(tok_hbm, tok_ref, load_sems.at[1])
     tok_load.start()
     loads = [
-        pltpu.make_async_copy(w, weights.at[i], load_sems.at[i])
+        pltpu.make_async_copy(w, weights.at[i], load_sems.at[0])
         for i, w in enumerate((key_w_hbm, value_w_hbm, lru_w_hbm, query_w_hbm, gate_w_hbm))
     ]
     own_blocks = pl.ds(2 * tp, 2)
     own_columns = pl.ds(pl.multiple_of(tp * OUT, OUT), OUT)
     later_loads = [
-        pltpu.make_async_copy(extra_hbm, extra_ref, load_sems.at[6]),
-        pltpu.make_async_copy(recur_hbm.at[own_blocks], recur_ref, load_sems.at[7]),
-        pltpu.make_async_copy(input_hbm.at[own_blocks], input_ref, load_sems.at[8]),
-        pltpu.make_async_copy(out_lru_ref.at[:, own_columns], w_out.at[0, tp], load_sems.at[9]),
-        pltpu.make_async_copy(out_fox_ref.at[:, own_columns], w_out.at[1, tp], load_sems.at[10]),
+        pltpu.make_async_copy(extra_hbm, extra_ref, load_sems.at[2]),
+        pltpu.make_async_copy(recur_hbm.at[own_blocks], recur_ref, load_sems.at[3]),
+        pltpu.make_async_copy(input_hbm.at[own_blocks], input_ref, load_sems.at[4]),
+        pltpu.make_async_copy(out_lru_ref.at[:, own_columns], w_out.at[0, tp], load_sems.at[5]),
+        pltpu.make_async_copy(out_fox_ref.at[:, own_columns], w_out.at[1, tp], load_sems.at[6]),
     ]
     for load in loads + later_loads:
         load.start()
@@ -219,7 +232,7 @@
         tell(alive, sp=preceding)
 
     tokens = [
-        Gather(copy, tok_ref, tokg, along_y(1, c), along_y(3, c), partner, h * HALF, HALF) for h in (0, 1)
+        Gather(copy, gather_sems[h], tok_ref, tokg, along_y(1, c), along_y(3, c), partner, h * HALF, HALF) for h in (0, 1)
     ]
     tok_load.wait()
     tokens[0].begin()
@@ -287,9 +300,11 @@
 
     tail = copy(lru_own.at[pl.ds(BLK - 16, 16)], halo, sp=following)
     query_rows = [pl.ds(pl.multiple_of(x * BLK + h * HALF, HALF), HALF) for h in (0, 1)]
+    query_sems = semaphore(), semaphore()
     query_copies = [
-        {r: copy(qb.at[rows], qb.at[rows], sp=along_x(r)) for r in (1, 2, 3)} for rows in query_rows
+        {r: copy(qb.at[rows], qb.at[rows], *query_sems, sp=along_x(r)) for r in (1, 2, 3)} for rows in query_rows
     ]
+    others_queries = qb.at[pl.ds(0, (XS - 1) * BLK)]
 
     def conclude(h):
         half = pl.ds(h * HALF, HALF)
@@ -324,41 +339,45 @@
         for r in (1, 3, 2):
             query_copies[h][r].start()
 
-    for load in loads:
-        load.wait()
+    await_bytes(weights, load_sems.at[0])
     early, late = tokens
     early.arrived(0)
     take(0, 0)
     early.relay_first()
     late.begin()
     early.relay_second()
-    early.arrived(7, 8)
+    early.arrived_from_partner(4)
     take(1, 0)
-    early.arrived(9, 10)
+    early.arrived_from_partner(5)
     take(2, 0)
     early.relay_last()
     late.arrived(0)
     take(0, 1)
     late.relay_first()
-    early.arrived(11, 12)
+    early.arrived_from_partner(6)
     conclude(0)
     late.relay_second()
-    late.arrived(7, 8)
+    late.arrived_from_partner(4)
     take(1, 1)
-    late.arrived(9, 10)
+    late.arrived_from_partner(5)
     take(2, 1)
     late.relay_last()
-    late.arrived(11, 12)
+    late.arrived_from_partner(6)
     conclude(1)
 
+    for group in tokens:
+        group.finish()
+
+    weight_sems = semaphore(), semaphore()
     weight_copies = []
     for r in range(1, TP):
         to = lax.rem(tp + r, TP)
         columns = pl.ds(pl.multiple_of(to * OUT, OUT), OUT)
         for k, ref in enumerate((out_lru_ref, out_fox_ref)):
-            weight_copies.append(copy(ref.at[:, columns], w_out.at[k, tp], tp=to))
+            weight_copies.append(copy(ref.at[:, columns], w_out.at[k, tp], *weight_sems, tp=to))
     for each in weight_copies:
         each.start()
+    others_weights = w_out.at[:, pl.ds(0, TP - 1)]
     own_rows = pl.ds(pl.multiple_of(x * BLK, BLK), BLK)
     m_ref[...] = jnp.full_like(m_ref, NEG)
     l_ref[...] = jnp.zeros_like(l_ref)
@@ -451,14 +470,6 @@
 
     def take_keys(i):
         d = i // 2 + 1
-        if d == 4:
-
-            @pl.when(z >= 4)
-            def _():
-                visit(14, 15)
-
-            return
-
         @pl.when(z + d >= ZS)
         def _():
             visit(i + 2, i + 8)
@@ -527,23 +538,24 @@
         return jnp.concatenate([a, b, jnp.zeros((6, 128), jnp.float32)], axis=0)
 
     row_tiles[0] = tile_of(decays[BLK - 1 :, :], drives[BLK - 1 :, :])
-    row_copies = {r: copy(row_tiles.at[0], row_tiles.at[r], sp=along_x(r)) for r in (1, 2, 3)}
+    row_sems = semaphore(), semaphore()
+    row_copies = {
+        r: copy(row_tiles.at[0], row_tiles.at[r], *row_sems, sp=along_x(r)) for r in (1, 2, 3)
+    }
+    others_rows = row_tiles.at[pl.ds(1, XS - 1)]
     for r in (1, 3, 2):
         row_copies[r].start()
 
     receive(1)
-    for queries in query_copies:
-        for r in (1, 3, 2):
-            queries[r].wait_recv()
+    await_bytes(others_queries, query_sems[1])
     visit_rest((0, 1), x + 1)
 
     column_copies = {r: copy(col_tiles.at[0], col_tiles.at[r], sp=along_z(r)) for r in range(1, ZS)}
-    branch = Gather(copy, lru_out, lru_g, along_y(1, c), along_y(3, c), partner)
+    branch = Gather(copy, gather_sems[0], lru_out, lru_g, along_y(1, c), along_y(3, c), partner)
     one, zero = jnp.ones((1, 128), jnp.float32), jnp.zeros((1, 128), jnp.float32)
 
     def total_of_row():
-        for r in (1, 3, 2):
-            row_copies[r].wait_recv()
+        await_bytes(others_rows, row_sems[1])
         whole_decay, whole_state, state = one, zero, zero
         for k in range(XS):
             block = row_tiles[lax.rem(x + XS - k, XS)]
@@ -580,7 +592,7 @@
         branch.begin()
 
     beside = {0: total_of_row, 2: recurrence_out, 4: branch.relay}
-    for i in range(7):
+    for i in range(6):
         take_keys(i)
         if i in beside:
             beside[i]()
@@ -592,6 +604,8 @@
             receive(7)
 
     right, left = along_x(1), along_x(3)
+    out_sent, out_sent_on = semaphore(), semaphore()
+    relay_sems, out_sems = [semaphore(), semaphore()], [semaphore(), semaphore()]
     out_copies = []
     for h in (0, 1):
         rows = pl.ds(h * HALF, HALF)
@@ -599,50 +613,68 @@
         out_copies.append(
             {
                 "relay": [
-                    copy(o_send.at[2, part], o_relay.at[k, part], sp=to)
+                    copy(o_send.at[2, part], o_relay.at[k, part], out_sent, relay_sems[h], sp=to)
                     for k, (part, to) in enumerate(zip(quarters, (right, left)))
                 ],
-                "near": [copy(o_send.at[r, rows], o_recv.at[r, rows], sp=along_x(r)) for r in (1, 3)],
+                "near": {
+                    r: copy(o_send.at[r, rows], o_recv.at[r, rows], out_sent, out_sems[h], sp=along_x(r))
+                    for r in (1, 3)
+                },
                 "far": [
-                    copy(o_relay.at[k, part], o_recv.at[2, part], sp=to)
+                    copy(o_relay.at[k, part], o_recv.at[2, part], out_sent_on, out_sems[h], sp=to)
                     for k, (part, to) in enumerate(zip(quarters, (right, left)))
                 ],
             }
         )
-    stat_copies = [copy(st_send.at[r], st_recv.at[r], sp=along_x(r)) for r in (1, 2, 3)]
+    stat_sems = semaphore(), semaphore()
+    stat_copies = {r: copy(st_send.at[r], st_recv.at[r], *stat_sems, sp=along_x(r)) for r in (1, 2, 3)}
+    others_stats = st_recv.at[pl.ds(1, XS - 1)]
 
     def stats(rows):
         total = jnp.broadcast_to(jnp.sum(l_ref[rows, :], axis=1, keepdims=True), (BLK, 128))
         return packed_rows(m_ref[rows, :]), packed_rows(total)
 
-    def send_out(h, kind):
-        for each in out_copies[h][kind]:
+    def relay_on(h):
+        await_bytes(o_relay.at[0, pl.ds(0, HALF)], relay_sems[h])
+        for each in out_copies[h]["far"]:
             each.start()
 
-    def got_out(h, kind):
-        for each in out_copies[h][kind]:
-            each.wait_recv()
-
-    def rows_of(r):
-        return pl.ds(pl.multiple_of(lax.rem(x + r, XS) * BLK, BLK), BLK)
-
-    o_send[2] = acc[rows_of(2), :].astype(jnp.bfloat16)
-    send_out(0, "relay")
-    for r in (1, 3):
-        o_send[r] = acc[rows_of(r), :].astype(jnp.bfloat16)
-    send_out(0, "near")
-    send_out(1, "relay")
-    for r in (1, 2, 3):
-        st_send[r] = jnp.concatenate(stats(rows_of(r)), axis=0)
-    for each in stat_copies:
-        each.start()
+    def block_of(r):
+        return lax.rem(x + r, XS)
+
+    @pl.when(z >= 4)
+    def _():
+        set_bias(14)
+        set_bias(15)
+        score(scores_a, block_of(2), (14, 15))
+
+    buffers = (scores_a, scores_b)
+    turns = (2, 1, 3, 0)
+    for k, r in enumerate(turns):
+
+        @pl.when(z >= 4)
+        def _():
+            if k + 1 < len(turns):
+                score(buffers[(k + 1) % 2], block_of(turns[k + 1]), (14, 15))
+            absorb(buffers[k % 2], block_of(r), (14, 15))
+
+        if r > 0:
+            rows = pl.ds(pl.multiple_of(block_of(r) * BLK, BLK), BLK)
+            o_send[r] = acc[rows, :].astype(jnp.bfloat16)
+            if r == 2:
+                for h in (0, 1):
+                    for each in out_copies[h]["relay"]:
+                        each.start()
+            else:
+                for h in (0, 1):
+                    out_copies[h]["near"][r].start()
+            st_send[r] = jnp.concatenate(stats(rows), axis=0)
+            stat_copies[r].start()
     tops, sums = [None] * 4, [None] * 4
     tops[0], sums[0] = stats(own_rows)
     branch.relay_last()
 
-    got_out(0, "relay")
-    send_out(0, "far")
-    send_out(1, "near")
+    relay_on(0)
 
     sources = [(0, c), (0, 1 - c), (3, c), (3, 1 - c), (1, c), (1, 1 - c), (2, c), (2, 1 - c)]
 
@@ -652,15 +684,13 @@
         rights = [w_out[k, along_y(*sources[i])] for i in which]
         return dot(jnp.concatenate(blocks, axis=1), jnp.concatenate(rights, axis=0))
 
-    for each in weight_copies:
-        each.wait_recv()
-    branch.arrived(0, 7, 8, 9, 10, 11, 12)
-    got_out(1, "relay")
-    send_out(1, "far")
+    await_bytes(others_weights, weight_sems[1])
+    branch.arrived(0)
+    branch.arrived_from_partner(4, 5, 6)
+    relay_on(1)
     acc_out[...] = branch_product(0, lru_out, lru_g, range(8), pl.ds(0, BLK))
 
-    for each in stat_copies:
-        each.wait_recv()
+    await_bytes(others_stats, stat_sems[1])
     for r in (1, 2, 3):
         both = st_recv[r]
         tops[r], sums[r] = both[0:4], both[4:8]
@@ -669,12 +699,11 @@
     whole = shares[0] * sums[0] + shares[1] * sums[1] + shares[2] * sums[2] + shares[3] * sums[3]
     shares = [s / whole for s in shares]
     heads = [
-        Gather(copy, fox_out, fox_g, along_y(1, c), along_y(3, c), partner, h * HALF, HALF) for h in (0, 1)
+        Gather(copy, gather_sems[1 + h], fox_out, fox_g, along_y(1, c), along_y(3, c), partner, h * HALF, HALF) for h in (0, 1)
     ]
 
     def merge(h):
-        got_out(h, "near")
-        got_out(h, "far")
+        await_bytes(qb.at[pl.ds(0, (XS - 1) * HALF)], out_sems[h])
         for g in (2 * h, 2 * h + 1):
             part = pl.ds(g * 128, 128)
             mine = pl.ds(pl.multiple_of(x * BLK + g * 128, 128), 128)
@@ -690,12 +719,12 @@
 
     halves = [pl.ds(h * HALF, HALF) for h in (0, 1)]
     out_loads = [
-        pltpu.make_async_copy(out_rows.at[half], o_ref.at[half], load_sems.at[11 + h])
+        pltpu.make_async_copy(out_rows.at[half], o_ref.at[half], load_sems.at[7 + h])
         for h, half in enumerate(halves)
     ]
 
     def write(h):
-        heads[h].arrived(11, 12)
+        heads[h].arrived_from_partner(6)
         out_rows[halves[h], :] = (acc_out[halves[h], :] + head_product(h, (6, 7))).astype(out_rows.dtype)
         out_loads[h].start()
 
@@ -709,11 +738,11 @@
     heads[1].relay_second()
     heads[1].arrived(0)
     acc_out[halves[1], :] += head_product(1, (0, 1))
-    heads[0].arrived(7, 8, 9, 10)
+    heads[0].arrived_from_partner(4, 5)
     acc_out[halves[0], :] += head_product(0, (2, 3, 4, 5))
     write(0)
     heads[1].relay_last()
-    heads[1].arrived(7, 8, 9, 10)
+    heads[1].arrived_from_partner(4, 5)
     acc_out[halves[1], :] += head_product(1, (2, 3, 4, 5))
     write(1)
 
@@ -739,16 +768,13 @@
         def _():
             column_copies[r].wait_send()
 
-    for each in weight_copies + stat_copies:
-        each.wait_send()
-    for group in query_copies + [row_copies]:
-        for each in group.values():
-            each.wait_send()
-    for group in out_copies:
-        for kind in group.values():
-            for each in kind:
-                each.wait_send()
-    for group in tokens + [branch] + heads:
+    await_bytes(others_weights, weight_sems[0])
+    await_bytes(others_queries, query_sems[0])
+    await_bytes(others_rows, row_sems[0])
+    await_bytes(others_stats, stat_sems[0])
+    await_bytes(o_recv.at[pl.ds(1, XS - 1)], out_sent)
+    await_bytes(o_relay.at[0], out_sent_on)
+    for group in [branch] + heads:
         group.finish()
     for each in out_loads:
         each.wait()
@@ -763,7 +789,7 @@
     bf16, f32 = jnp.bfloat16, jnp.float32
     return pl.pallas_call(
         layer_kernel,
-        out_shape=jax.ShapeDtypeStruct((BLK, OUT), bf16),
+        out_shape=jax.ShapeDtypeStruct((BLK, OUT), f32),
         in_specs=[hbm] * 6 + [vmem, hbm, hbm, vmem, hbm, vmem, hbm, hbm],
         out_specs=hbm,
         scratch_shapes=[
@@ -802,10 +828,9 @@
             pltpu.VMEM((7, BLK, 128), bf16),
             pltpu.VMEM((2, TP, 128, OUT), bf16),
             pltpu.VMEM((BLK, OUT), f32),
-            pltpu.VMEM((BLK, OUT), bf16),
+            pltpu.VMEM((BLK, OUT), f32),
             pltpu.SemaphoreType.DMA((COPIES,)),
-            pltpu.SemaphoreType.DMA((COPIES,)),
-            pltpu.SemaphoreType.DMA((13,)),
+            pltpu.SemaphoreType.DMA((9,)),
             pltpu.SemaphoreType.REGULAR,
         ],
         compiler_params=pltpu.CompilerParams(collective_id=1, has_side_effects=True),
@@ -813,7 +838,7 @@
     )(
         tokens, lru_in, lru_gate_in, query_w, key_w, value_w, conv_weight, recur_gate_w, input_gate_w,
         rate_param.reshape(TP, 128), decay_extra, forget_cum.reshape(4, 128), out_lru, out_fox,
-    )
+    ).astype(bf16)
 
 
 def solution(mesh):

time: 67 us -> 62.9 us (0.939)
  Pallas kernels: 65.1 us -> 60.9 us
  other arithmetic: 0 us -> 1.77 us
  local copies, waits for them, and re-layouts: 1.67 us -> 0 us
    pallas_call x1, Pallas kernels: 65.1 us -> 60.9 us  [layer(): pl.pallas_call(layer_kernel, out_shape=jax.ShapeDtypeStruct((BLK, OUT), f...]
    convert_element_type x0 -> x1, other arithmetic: none -> 1.77 us  [layer(): return pl.pallas_call(layer_kernel, out_shape=jax.ShapeDtypeStruct((BLK,...]
    unnamed x1 -> x0, local copies, waits for them, and re-layouts: 1.67 us -> none
where the time goes in v5:
time: 62.9 us; the launch traced here: 62.7 us
  Pallas kernels  60.9 us (97%)
  other arithmetic  1.77 us (3%)
    pallas_call x1, Pallas kernels, layer(): pl.pallas_call(layer_kernel, out_shape=jax.ShapeDtypeStruct((BLK, OUT), f...  60.9 us
    convert_element_type x1, other arithmetic, layer(): return pl.pallas_call(layer_kernel, out_shape=jax.ShapeDtypeStruct((BLK,...  1.77 us

profile of v5, /device:TPU:193, one launch (start us, length us, event | category | flops | bytes accessed | tf_op | source)
XLA Modules:
  0.0 62.7 jit_solution(3649396950359932726)
XLA Ops:
  0.0 60.9 %shard_map.136 = f32[512,256]{1,0:T(8,128)} custom-call(bf16[512,256]{1,0:T(8,128)(2,1)} %tok_hbm.1, bf16[2048,128]{1,0:T(8,128)(2,1)} %lru_w_hbm.1, bf16[2048,128]{1,0:T(8,128)(2,1)} %gate_w_hbm.1, bf16[2048,128]{1,0:T(8,128)(2,1)} %query_w_hbm.1, bf16[2048,128]{1,0:T(8,128)(2,1)} %key_w_hbm.1, bf16[2048,128]{1,0:T(8,128)(2,1)} %value_w_hbm.1, ...), custom_call_target="tpu_custom_call" | custom-call | flops 5000000000 | bytes 8000000 | tf_op jit(solution)/shard_map/pallas_call | solution.py:790
  60.9 1.8 %convert_element_type.3 = bf16[512,256]{1,0:T(8,128)(2,1)} convert(f32[512,256]{1,0:T(8,128)} %shard_map.136) | non-fusion elementwise | flops 131072 | bytes 786432 | tf_op jit(solution)/shard_map/convert_element_type | solution.py:841

commit v6 on v5

--- a/solution.py
+++ b/solution.py
@@ -19,6 +19,7 @@
 LOG2E = 1.4426950408889634
 NEG = -1e30
 COPIES = 96
+ROWS = 256
 
 decay_sharpness = 8.0
 epsilon_norm = 1e-06
@@ -144,7 +145,7 @@
     conv_ref, recur_hbm, input_hbm, rate_ref, extra_hbm, f_ref, out_lru_ref, out_fox_ref,
     o_ref,
     tok_ref, recur_ref, input_ref, extra_ref, weights, tokg, acc_kv, acc_rest, scores_a, scores_b, squares,
-    kv, qb, bias, m_ref, l_ref, acc, o_send, st_send, o_relay, o_recv, st_recv,
+    kv, qb, bias, m_ref, acc, o_send, st_send, o_relay, o_recv, st_recv,
     lru_own, halo, gate_own, decays, drives, row_tiles, col_tiles,
     lru_out, lru_g, fox_out, fox_g, w_out, acc_out, out_rows,
     copy_sems, load_sems, alive,
@@ -297,6 +298,30 @@
         @pl.when(wrapped(i // 2))
         def _():
             minus[i].start()
+
+    last_row = z == ZS - 1
+
+    def receive_plus(i, where=True):
+        d = i // 2 + 1
+
+        @pl.when((z >= d) & where)
+        def _():
+            plus[i].wait_recv()
+
+        if d < 3:
+
+            @pl.when((z < ZS - 1) & (z >= d) & where)
+            def _():
+                plus[i + 2].start()
+
+    def receive_minus(i, where=True):
+        d = i // 2 + 1
+
+        @pl.when(wrapped(d) & where)
+        def _():
+            minus[i].wait_recv()
+            if d < 4:
+                minus[i + 2].start()
 
     tail = copy(lru_own.at[pl.ds(BLK - 16, 16)], halo, sp=following)
     query_rows = [pl.ds(pl.multiple_of(x * BLK + h * HALF, HALF), HALF) for h in (0, 1)]
@@ -361,6 +386,7 @@
     take(1, 1)
     late.arrived_from_partner(5)
     take(2, 1)
+    receive_minus(0, last_row)
     late.relay_last()
     late.arrived_from_partner(6)
     conclude(1)
@@ -380,7 +406,6 @@
     others_weights = w_out.at[:, pl.ds(0, TP - 1)]
     own_rows = pl.ds(pl.multiple_of(x * BLK, BLK), BLK)
     m_ref[...] = jnp.full_like(m_ref, NEG)
-    l_ref[...] = jnp.zeros_like(l_ref)
     acc[...] = jnp.zeros_like(acc)
 
     def set_bias(slot):
@@ -395,7 +420,7 @@
         return parts[0] if len(parts) == 1 else jnp.concatenate(parts, axis=axis)
 
     def score(buffer, i, slots):
-        rows = pl.ds(pl.multiple_of(i * BLK, BLK), BLK)
+        rows = pl.ds(i * BLK if isinstance(i, int) else pl.multiple_of(i * BLK, BLK), BLK)
         buffer[:, : HALF * len(slots)] = lax.dot_general(
             qb[rows, :],
             joint([kv[slot, :HALF, :] for slot in slots], 0),
@@ -404,27 +429,27 @@
         )
 
     def absorb(buffer, i, slots, masked=False):
-        rows = pl.ds(pl.multiple_of(i * BLK, BLK), BLK)
         width = HALF * len(slots)
         offsets = joint([bias[slot : slot + 1, :] for slot in slots], 1)
-        scores = buffer[:, :width] * scale + offsets
-        if masked:
-            earlier = lax.broadcasted_iota(jnp.int32, scores.shape, 0) >= lax.broadcasted_iota(
-                jnp.int32, scores.shape, 1
+        values = joint([kv[slot, HROWS:, :] for slot in slots], 0)
+        values = jnp.concatenate([values, jnp.ones_like(values)], axis=1)
+        start = i * BLK if isinstance(i, int) else pl.multiple_of(i * BLK, BLK)
+        for part in range(0, BLK, ROWS):
+            rows = pl.ds(start + part, ROWS)
+            scores = buffer[part : part + ROWS, :width] * scale + offsets
+            if masked:
+                earlier = lax.broadcasted_iota(jnp.int32, scores.shape, 0) + part >= (
+                    lax.broadcasted_iota(jnp.int32, scores.shape, 1)
+                )
+                scores = jnp.where(earlier, scores, NEG)
+            old = m_ref[rows, :]
+            new = jnp.maximum(old, jnp.max(scores, axis=1, keepdims=True))
+            rescale = jnp.exp2(old - new)
+            probs = jnp.exp2(scores - jnp.concatenate([new] * (width // 128), axis=1))
+            m_ref[rows, :] = new
+            acc[rows, :] = acc[rows, :] * jnp.concatenate([rescale] * 2, axis=1) + dot(
+                probs.astype(jnp.bfloat16), values
             )
-            scores = jnp.where(earlier, scores, NEG)
-        old = m_ref[rows, :]
-        new = jnp.maximum(old, jnp.max(scores, axis=1, keepdims=True))
-        rescale = jnp.exp2(old - new)
-        probs = jnp.exp2(scores - jnp.concatenate([new] * (width // 128), axis=1))
-        total = l_ref[rows, :] * rescale
-        for g in range(width // 128):
-            total = total + probs[:, g * 128 : (g + 1) * 128]
-        l_ref[rows, :] = total
-        m_ref[rows, :] = new
-        acc[rows, :] = acc[rows, :] * rescale + dot(
-            probs.astype(jnp.bfloat16), joint([kv[slot, HROWS:, :] for slot in slots], 0)
-        )
 
     def attend(i, slots, masked=False):
         score(scores_a, i, slots)
@@ -441,32 +466,11 @@
         for slot in slots:
             set_bias(slot)
         score(scores_a, 0, slots)
-
-        def body(k, carry):
-            score(scores_b, 2 * k + 1, slots)
-            absorb(scores_a, 2 * k, slots)
-            score(scores_a, jnp.minimum(2 * k + 2, XS - 1), slots)
-            absorb(scores_b, 2 * k + 1, slots)
-            return carry
-
-        lax.fori_loop(0, XS // 2, body, 0)
-
-    def receive(i):
-        d = i // 2 + 1
-        if d < 4:
-
-            @pl.when(z >= d)
-            def _():
-                plus[i].wait_recv()
-
-            if d < 3:
-                send_plus(i + 2)
-
-        @pl.when(wrapped(d))
-        def _():
-            minus[i].wait_recv()
-            if d < 4:
-                minus[i + 2].start()
+        pair = scores_a, scores_b
+        for k in range(XS):
+            if k + 1 < XS:
+                score(pair[(k + 1) % 2], k + 1, slots)
+            absorb(pair[k % 2], k, slots)
 
     def take_keys(i):
         d = i // 2 + 1
@@ -481,7 +485,9 @@
     set_bias(0)
     set_bias(1)
     attend(x, (0, 1), masked=True)
-    receive(0)
+    receive_plus(0)
+    receive_minus(0, z < ZS - 1)
+    receive_minus(1, last_row)
 
     @pl.when(sp > 0)
     def _():
@@ -546,7 +552,9 @@
     for r in (1, 3, 2):
         row_copies[r].start()
 
-    receive(1)
+    receive_minus(1, z < ZS - 1)
+    receive_plus(1, z < ZS - 1)
+    receive_minus(2, z >= ZS - 2)
     await_bytes(others_queries, query_sems[1])
     visit_rest((0, 1), x + 1)
 
@@ -592,16 +600,17 @@
         branch.begin()
 
     beside = {0: total_of_row, 2: recurrence_out, 4: branch.relay}
+    receive_minus(2, z < ZS - 2)
     for i in range(6):
         take_keys(i)
         if i in beside:
             beside[i]()
+        if i == 0:
+            receive_plus(1, last_row)
         if i < 4:
-            receive(i + 2)
-        elif i == 4:
-            receive(6)
-        elif i == 5:
-            receive(7)
+            receive_plus(i + 2)
+        if i < 5:
+            receive_minus(i + 3)
 
     right, left = along_x(1), along_x(3)
     out_sent, out_sent_on = semaphore(), semaphore()
@@ -631,8 +640,7 @@
     others_stats = st_recv.at[pl.ds(1, XS - 1)]
 
     def stats(rows):
-        total = jnp.broadcast_to(jnp.sum(l_ref[rows, :], axis=1, keepdims=True), (BLK, 128))
-        return packed_rows(m_ref[rows, :]), packed_rows(total)
+        return packed_rows(m_ref[rows, :]), packed_rows(acc[rows, 128:])
 
     def relay_on(h):
         await_bytes(o_relay.at[0, pl.ds(0, HALF)], relay_sems[h])
@@ -660,7 +668,9 @@
 
         if r > 0:
             rows = pl.ds(pl.multiple_of(block_of(r) * BLK, BLK), BLK)
-            o_send[r] = acc[rows, :].astype(jnp.bfloat16)
+            st_send[r] = jnp.concatenate(stats(rows), axis=0)
+            stat_copies[r].start()
+            o_send[r] = acc[rows, :128].astype(jnp.bfloat16)
             if r == 2:
                 for h in (0, 1):
                     for each in out_copies[h]["relay"]:
@@ -668,8 +678,6 @@
             else:
                 for h in (0, 1):
                     out_copies[h]["near"][r].start()
-            st_send[r] = jnp.concatenate(stats(rows), axis=0)
-            stat_copies[r].start()
     tops, sums = [None] * 4, [None] * 4
     tops[0], sums[0] = stats(own_rows)
     branch.relay_last()
@@ -707,7 +715,7 @@
         for g in (2 * h, 2 * h + 1):
             part = pl.ds(g * 128, 128)
             mine = pl.ds(pl.multiple_of(x * BLK + g * 128, 128), 128)
-            total = unpacked_row(shares[0][g : g + 1]) * acc[mine, :]
+            total = unpacked_row(shares[0][g : g + 1]) * acc[mine, :128]
             for r in (1, 2, 3):
                 total = total + unpacked_row(shares[r][g : g + 1]) * o_recv[r, part, :].astype(jnp.float32)
             fox_out[part, :] = total.astype(jnp.bfloat16)
@@ -808,8 +816,7 @@
             pltpu.VMEM((XS * BLK, 128), bf16),
             pltpu.VMEM((2 * ZS, HALF), f32),
             pltpu.VMEM((XS * BLK, 128), f32),
-            pltpu.VMEM((XS * BLK, 128), f32),
-            pltpu.VMEM((XS * BLK, 128), f32),
+            pltpu.VMEM((XS * BLK, 256), f32),
             pltpu.VMEM((XS, BLK, 128), bf16),
             pltpu.VMEM((XS, 8, 128), f32),
             pltpu.VMEM((2, BLK, 128), bf16),

time: 62.9 us -> 61.5 us (0.978)
  Pallas kernels: 60.9 us -> 59.6 us
    pallas_call x1, Pallas kernels: 60.9 us -> 59.6 us  [layer(): pl.pallas_call(layer_kernel, out_shape=jax.ShapeDtypeStruct((BLK, OUT), f...]
where the time goes in v6:
time: 61.5 us; the launch traced here: 61.3 us
  Pallas kernels  59.6 us (97%)
  other arithmetic  1.77 us (3%)
    pallas_call x1, Pallas kernels, layer(): pl.pallas_call(layer_kernel, out_shape=jax.ShapeDtypeStruct((BLK, OUT), f...  59.6 us
    convert_element_type x1, other arithmetic, layer(): return pl.pallas_call(layer_kernel, out_shape=jax.ShapeDtypeStruct((BLK,...  1.77 us

profile of v6, /device:TPU:193, one launch (start us, length us, event | category | flops | bytes accessed | tf_op | source)
XLA Modules:
  0.0 61.3 jit_solution(4614125969569147931)
XLA Ops:
  0.0 59.6 %shard_map.136 = f32[512,256]{1,0:T(8,128)} custom-call(bf16[512,256]{1,0:T(8,128)(2,1)} %tok_hbm.1, bf16[2048,128]{1,0:T(8,128)(2,1)} %lru_w_hbm.1, bf16[2048,128]{1,0:T(8,128)(2,1)} %gate_w_hbm.1, bf16[2048,128]{1,0:T(8,128)(2,1)} %query_w_hbm.1, bf16[2048,128]{1,0:T(8,128)(2,1)} %key_w_hbm.1, bf16[2048,128]{1,0:T(8,128)(2,1)} %value_w_hbm.1, ...), custom_call_target="tpu_custom_call" | custom-call | flops 5000000000 | bytes 8000000 | tf_op jit(solution)/shard_map/pallas_call | solution.py:798
  59.6 1.8 %convert_element_type.3 = bf16[512,256]{1,0:T(8,128)(2,1)} convert(f32[512,256]{1,0:T(8,128)} %shard_map.136) | non-fusion elementwise | flops 131072 | bytes 786432 | tf_op jit(solution)/shard_map/convert_element_type | solution.py:848

commit v7 on v6

--- a/solution.py
+++ b/solution.py
@@ -73,7 +73,7 @@
 
 
 class Gather:
-    def __init__(self, copy, sems, own, slots, up, down, partner, start=0, rows=BLK):
+    def __init__(self, copy, sems, own, slots, up, down, partner, start=0, rows=BLK, last=None):
         half = rows // 2
         first, second = pl.ds(start, half), pl.ds(start + half, half)
 
@@ -93,9 +93,10 @@
             (1, 4, second, partner, 7),
             (2, 5, first, partner, 8),
             (2, 5, second, partner, 8),
-            (3, 6, first, partner, 9),
-            (3, 6, second, partner, 9),
+            (3, 6, first, partner, 9) if last is None else (1, 6, first, last[0], 9),
+            (3, 6, second, partner, 9) if last is None else (2, 6, second, last[1], 9),
         ]
+        self.direct = last is not None
         self.copies = [send(*each) for each in plan]
         self.sems, self.slots, self.rows = sems, slots, pl.ds(start, rows)
 
@@ -120,8 +121,12 @@
     def relay_first(self):
         self.arrived(1)
         self.start(5, 7)
+        if self.direct:
+            self.start(11)
         self.arrived(3)
         self.start(6, 10)
+        if self.direct:
+            self.start(12)
 
     def relay_second(self):
         self.arrived(2)
@@ -135,9 +140,11 @@
 
     def relay_last(self):
         self.arrived(5)
-        self.start(11)
+        if not self.direct:
+            self.start(11)
         self.arrived(6)
-        self.start(12)
+        if not self.direct:
+            self.start(12)
 
 
 def layer_kernel(
@@ -707,7 +714,11 @@
     whole = shares[0] * sums[0] + shares[1] * sums[1] + shares[2] * sums[2] + shares[3] * sums[3]
     shares = [s / whole for s in shares]
     heads = [
-        Gather(copy, gather_sems[1 + h], fox_out, fox_g, along_y(1, c), along_y(3, c), partner, h * HALF, HALF) for h in (0, 1)
+        Gather(
+            copy, gather_sems[1 + h], fox_out, fox_g, along_y(1, c), along_y(3, c), partner, h * HALF, HALF,
+            last=(along_y(1, 1 - c), along_y(3, 1 - c)),
+        )
+        for h in (0, 1)
     ]
 
     def merge(h):
@@ -797,7 +808,7 @@
     bf16, f32 = jnp.bfloat16, jnp.float32
     return pl.pallas_call(
         layer_kernel,
-        out_shape=jax.ShapeDtypeStruct((BLK, OUT), f32),
+        out_shape=pltpu.VMEM((BLK, OUT), f32),
         in_specs=[hbm] * 6 + [vmem, hbm, hbm, vmem, hbm, vmem, hbm, hbm],
         out_specs=hbm,
         scratch_shapes=[

time: 61.5 us -> 59.1 us (0.961)
  Pallas kernels: 59.6 us -> 58.2 us
  other arithmetic: 1.77 us -> 0.73 us
    pallas_call x1, Pallas kernels: 59.6 us -> 58.2 us  [layer(): pl.pallas_call(layer_kernel, out_shape=pltpu.VMEM((BLK, OUT), f32), in_sp...]
    convert_element_type x1, other arithmetic: 1.77 us -> 0.73 us  [layer(): return pl.pallas_call(layer_kernel, out_shape=pltpu.VMEM((BLK, OUT), f32)...]
where the time goes in v7:
time: 59.1 us; the launch traced here: 59 us
  Pallas kernels  58.2 us (98%)
  other arithmetic  0.73 us (1%)
    pallas_call x1, Pallas kernels, layer(): pl.pallas_call(layer_kernel, out_shape=pltpu.VMEM((BLK, OUT), f32), in_sp...  58.2 us

profile of v7, /device:TPU:193, one launch (start us, length us, event | category | flops | bytes accessed | tf_op | source)
XLA Modules:
  0.0 59.0 jit_solution(16835110651655259576)
XLA Ops:
  0.0 58.2 %shard_map.136 = f32[512,256]{1,0:T(8,128)S(1)} custom-call(bf16[512,256]{1,0:T(8,128)(2,1)} %tok_hbm.1, bf16[2048,128]{1,0:T(8,128)(2,1)} %lru_w_hbm.1, bf16[2048,128]{1,0:T(8,128)(2,1)} %gate_w_hbm.1, bf16[2048,128]{1,0:T(8,128)(2,1)} %query_w_hbm.1, bf16[2048,128]{1,0:T(8,128)(2,1)} %key_w_hbm.1, bf16[2048,128]{1,0:T(8,128)(2,1)} %value_w_hbm.1, ...), custom_call_target="tpu_custom_call" | custom-call | flops 5000000000 | bytes 8000000 | tf_op jit(solution)/shard_map/pallas_call | solution.py:809
  58.3 0.7 %convert_element_type.3 = bf16[512,256]{1,0:T(8,128)(2,1)} convert(f32[512,256]{1,0:T(8,128)S(1)} %shard_map.136) | non-fusion elementwise | flops 131072 | bytes 786432 | tf_op jit(solution)/shard_map/convert_element_type | solution.py:859

commit v8 on v7

--- a/solution.py
+++ b/solution.py
@@ -18,7 +18,7 @@
 PIECE = HROWS + HALF
 LOG2E = 1.4426950408889634
 NEG = -1e30
-COPIES = 96
+COPIES = 73
 ROWS = 256
 
 decay_sharpness = 8.0
@@ -290,8 +290,9 @@
 
     plus = [(0, 2), (1, 3), (2, 4), (3, 5), (4, 6), (5, 7)]
     minus = [(0, 8), (1, 9), (8, 10), (9, 11), (10, 12), (11, 13), (12, 14), (13, 15)]
-    plus = [copy(kv.at[a], kv.at[b], sp=above) for a, b in plus]
-    minus = [copy(kv.at[a], kv.at[b], sp=below) for a, b in minus]
+    plus_sent, minus_sent = semaphore(), semaphore()
+    plus = [copy(kv.at[a], kv.at[b], plus_sent, sp=above) for a, b in plus]
+    minus = [copy(kv.at[a], kv.at[b], minus_sent, sp=below) for a, b in minus]
 
     def wrapped(d):
         return lax.rem(z + d, ZS) < 4
@@ -565,7 +566,10 @@
     await_bytes(others_queries, query_sems[1])
     visit_rest((0, 1), x + 1)
 
-    column_copies = {r: copy(col_tiles.at[0], col_tiles.at[r], sp=along_z(r)) for r in range(1, ZS)}
+    columns_sent = semaphore()
+    column_copies = {
+        r: copy(col_tiles.at[0], col_tiles.at[r], columns_sent, sp=along_z(r)) for r in range(1, ZS)
+    }
     branch = Gather(copy, gather_sems[0], lru_out, lru_g, along_y(1, c), along_y(3, c), partner)
     one, zero = jnp.ones((1, 128), jnp.float32), jnp.zeros((1, 128), jnp.float32)
 
@@ -765,27 +769,27 @@
     acc_out[halves[1], :] += head_product(1, (2, 3, 4, 5))
     write(1)
 
-    for i, each in enumerate(plus):
-
-        @pl.when((z < ZS - 1) & (z >= i // 2))
-        def _():
-            each.wait_send()
-
-    for i, each in enumerate(minus):
-
-        @pl.when(wrapped(i // 2))
-        def _():
-            each.wait_send()
+    for n in (1, 2, 3):
+
+        @pl.when((z < ZS - 1) & (jnp.minimum(z + 1, 3) == n))
+        def _():
+            await_bytes(kv.at[pl.ds(0, 2 * n)], plus_sent)
+
+    for n in (1, 2, 3, 4):
+
+        @pl.when((z == 4 - n) | (z == 4 + n))
+        def _():
+            await_bytes(kv.at[pl.ds(0, 2 * n)], minus_sent)
 
     @pl.when(sp < SP - 1)
     def _():
         tail.wait_send()
 
-    for r in range(1, ZS):
-
-        @pl.when(z + r < ZS)
-        def _():
-            column_copies[r].wait_send()
+    for n in range(1, ZS):
+
+        @pl.when(z == ZS - 1 - n)
+        def _():
+            await_bytes(col_tiles.at[pl.ds(0, n)], columns_sent)
 
     await_bytes(others_weights, weight_sems[0])
     await_bytes(others_queries, query_sems[0])

time: 59.1 us -> 58.9 us (level)
  no operation moved by 1% of the time
where the time goes in v8:
time: 58.9 us; the launch traced here: 58.8 us
  Pallas kernels  58 us (98%)
  other arithmetic  0.73 us (1%)
    pallas_call x1, Pallas kernels, layer(): pl.pallas_call(layer_kernel, out_shape=pltpu.VMEM((BLK, OUT), f32), in_sp...  58 us

profile of v8, /device:TPU:193, one launch (start us, length us, event | category | flops | bytes accessed | tf_op | source)
XLA Modules:
  0.0 58.8 jit_solution(11238458767474450128)
XLA Ops:
  0.0 58.0 %shard_map.136 = f32[512,256]{1,0:T(8,128)S(1)} custom-call(bf16[512,256]{1,0:T(8,128)(2,1)} %tok_hbm.1, bf16[2048,128]{1,0:T(8,128)(2,1)} %lru_w_hbm.1, bf16[2048,128]{1,0:T(8,128)(2,1)} %gate_w_hbm.1, bf16[2048,128]{1,0:T(8,128)(2,1)} %query_w_hbm.1, bf16[2048,128]{1,0:T(8,128)(2,1)} %key_w_hbm.1, bf16[2048,128]{1,0:T(8,128)(2,1)} %value_w_hbm.1, ...), custom_call_target="tpu_custom_call" | custom-call | flops 5000000000 | bytes 8000000 | tf_op jit(solution)/shard_map/pallas_call | solution.py:813
  58.0 0.7 %convert_element_type.3 = bf16[512,256]{1,0:T(8,128)(2,1)} convert(f32[512,256]{1,0:T(8,128)S(1)} %shard_map.136) | non-fusion elementwise | flops 131072 | bytes 786432 | tf_op jit(solution)/shard_map/convert_element_type | solution.py:863
